TPU v7x, 256 devices: a whole 4x4x8 slice. The times are simulated.
256 devices in a mesh: sp: 32 (over z, x), tp: 8 (over y, core).
Axes of the slice: x: 4, y: 4, z: 8, core: 2. Of those that a mesh axis runs over, the one named last changes fastest.
Arguments:
- token_grid: bfloat16 [32, 2048, 512], P('sp', 'tp'), may hold values from -6 to 6
- norm_gain: bfloat16 [3, 2048], replicated, may hold values from 0.099609375 to 1.8984375
- w_query: bfloat16 [3, 2048, 2048], P(None, None, 'tp'), may hold values from -0.125 to 0.125
- w_key: bfloat16 [3, 2048, 2048], P(None, None, 'tp'), may hold values from -0.125 to 0.125
- w_value: bfloat16 [3, 2048, 2048], P(None, None, 'tp'), may hold values from -0.125 to 0.125
- w_out: bfloat16 [3, 2048, 2048], P(None, 'tp'), may hold values from -0.5 to 0.5
- rel_bias: float32 [3, 32, 8, 16], P(None, 'tp'), may hold values from -3 to 250
Outputs:
- grid_out: bfloat16 [32, 2048, 512], P('sp', 'tp')
All inputs are finite; a program needn't handle non-finite values.
Results may differ from a plain program's by a relative error of at most 0.024.
Values may be sent and summed in bfloat16 or wider, within the bound.
A program may use at most 128 MiB of HBM per device.

v0:
```python
import jax
import jax.numpy as jnp
from jax import lax
from jax.sharding import PartitionSpec as P

D = 2048
HEAD_DIM = 64
WIN_R = 8
WIN_C = 16
LAYERS = 3


EPS = 1e-06


def copy_for_each(x, axis):
    size = lax.axis_size(axis)
    return lax.all_to_all(jnp.broadcast_to(x[None], (size, *x.shape)), axis, 0, 0, tiled=True)


def laid_out(pieces, dim):
    lengths = list(pieces.shape[1:])
    lengths[dim] *= pieces.shape[0]
    return jnp.moveaxis(pieces, 0, dim).reshape(lengths)


def collect(x, axis, dim):
    pieces = copy_for_each(x, axis)
    return laid_out(pieces, dim)


def from_behind(block, axis, distance):
    devices = range(lax.axis_size(axis))
    route = [((i - distance) % len(devices), i) for i in devices]
    return lax.ppermute(block, axis, route)


def cut_along(x, dim, size):
    before, after = (x.shape[:dim], x.shape[dim + 1 :])
    return jnp.moveaxis(x.reshape(*before, size, -1, *after), dim, 0)


def sent_and_summed(x, axis, dim):
    pieces = cut_along(x, dim, lax.axis_size(axis))
    arrived = lax.all_to_all(pieces, axis, split_axis=0, concat_axis=0, tiled=True)
    return arrived.astype(jnp.float32).sum(axis=0)


def periodic(source, columns):
    half_c = WIN_C // 2
    return jnp.concatenate(
        [source[..., columns - half_c :], source, source[..., : WIN_C - half_c - 1]], axis=-1
    )


def body(token_grid, norm_gain, w_query, w_key, w_value, w_out, rel_bias):
    current = token_grid
    heads_dev = rel_bias.shape[1]
    channels = w_query.shape[2]
    columns = token_grid.shape[2]
    half_r = WIN_R // 2
    factor = HEAD_DIM ** (-0.5)
    for layer_idx in range(LAYERS):
        gain_row = norm_gain[layer_idx].astype(jnp.float32)
        rows_query = w_query[layer_idx]
        rows_key = w_key[layer_idx]
        rows_value = w_value[layer_idx]
        raw_rows = collect(current, "tp", 1)[0].astype(jnp.float32)
        scaled = (raw_rows * gain_row[:, None]).astype(jnp.bfloat16)
        slice_keyval = jnp.concatenate([rows_key, rows_value], axis=1)
        contract = (((0,), (0,)), ((), ()))
        acc_query = lax.dot_general(
            rows_query, scaled, contract, preferred_element_type=jnp.float32
        )
        acc_keyval = lax.dot_general(
            slice_keyval, scaled, contract, preferred_element_type=jnp.float32
        )
        squares = jnp.sum(raw_rows * raw_rows, axis=0)
        acc_query, acc_keyval, squares = (acc_query, acc_keyval, squares)
        inverse = lax.rsqrt(squares / D + EPS)
        queries = (acc_query * inverse[None, :]).astype(jnp.bfloat16)
        keyval = (acc_keyval * inverse[None, :]).astype(jnp.bfloat16)
        rows_list = []
        for slot_idx in range(WIN_R):
            distance = half_r - slot_idx
            if distance == 0:
                rows_list.append(keyval)
            else:
                rows_list.append(from_behind(keyval, "sp", distance))
        window_rows = jnp.stack(rows_list)
        key_rows = window_rows[:, :channels].reshape(WIN_R, heads_dev, HEAD_DIM, columns)
        value_rows = window_rows[:, channels:].reshape(WIN_R, heads_dev, HEAD_DIM, columns)
        query_heads = queries.reshape(heads_dev, HEAD_DIM, columns)
        bias_table = rel_bias[layer_idx]
        wide_keys = periodic(key_rows, columns)
        score_list = []
        for offset in range(WIN_C):
            shifted = wide_keys[..., offset : offset + columns]
            partial_value = jnp.einsum(
                "hdc,shdc->shc", query_heads, shifted, preferred_element_type=jnp.float32
            )
            score_list.append(
                partial_value * factor + jnp.transpose(bias_table[:, :, offset])[:, :, None]
            )
        scores = jnp.stack(score_list)
        highest = jnp.max(scores, axis=(0, 1), keepdims=True)
        weights = jnp.exp(scores - highest)
        weights = (weights / jnp.sum(weights, axis=(0, 1), keepdims=True)).astype(jnp.bfloat16)
        wide_values = periodic(value_rows, columns)
        mixed_out = jnp.zeros((heads_dev, HEAD_DIM, columns), jnp.float32)
        for offset in range(WIN_C):
            shifted = wide_values[..., offset : offset + columns]
            mixed_out = mixed_out + jnp.einsum(
                "shc,shdc->hdc", weights[offset], shifted, preferred_element_type=jnp.float32
            )
        mixed_out = mixed_out.reshape(channels, columns).astype(jnp.bfloat16)
        w_layer = w_out[layer_idx]
        update = sent_and_summed(
            lax.dot_general(
                w_layer, mixed_out, (((0,), (0,)), ((), ())), preferred_element_type=jnp.float32
            ).astype(jnp.bfloat16),
            "tp",
            0,
        )
        current = (current[0].astype(jnp.float32) + update).astype(jnp.bfloat16)[None]
    return current


def solution(mesh):
    in_specs = (
        P("sp", "tp", None),
        P(),
        P(None, None, "tp"),
        P(None, None, "tp"),
        P(None, None, "tp"),
        P(None, "tp", None),
        P(None, "tp", None, None),
    )
    out_specs = P("sp", "tp", None)
    return jax.shard_map(body, mesh=mesh, in_specs=in_specs, out_specs=out_specs, check_vma=False)
```

profile of v0, /device:TPU:1, one launch (start us, length us, event | category | flops | bytes accessed | tf_op | source)
XLA Modules:
  0.0 534.5 jit_solution(8552652771469217454)
XLA Ops:
  2.5 6.7 %all-to-all-start = ((bf16[8,1,256,512]{3,2,1,0:T(8,128)(2,1)}), bf16[8,1,256,512]{3,2,1,0:T(8,128)(2,1)S(1)}, u32[]{:S(2)}, u32[]{:S(2)}) async-start(bf16[8,1,256,512]{3,2,1,0:T(8,128)(2,1)} %broadcast_in_dim.9), calls=%async_computation | async-start | bytes 4194304 | tf_op jit(solution)/shard_map/all_to_all | solution.py:18
  9.3 5.2 slice_bitcast_fusion
  14.5 20.9 %all-to-all-done = bf16[8,1,256,512]{3,2,1,0:T(8,128)(2,1)S(1)} async-done(((bf16[8,1,256,512]{3,2,1,0:T(8,128)(2,1)}), bf16[8,1,256,512]{3,2,1,0:T(8,128)(2,1)S(1)}, u32[]{:S(2)}, u32[]{:S(2)}) %all-to-all-start) | async-done | bytes 2097184 | tf_op jit(solution)/shard_map/all_to_all | solution.py:18
  57.8 27.6 %collective-permute-done.1 = bf16[512,512]{1,0:T(8,128)(2,1)S(1)} collective-permute-done((bf16[512,512]{1,0:T(8,128)(2,1)S(1)}, bf16[512,512]{1,0:T(8,128)(2,1)S(1)}, u32[]{:S(2)}, u32[]{:S(2)}) %collective-permute-start.1) | collective-permute-done | bytes 524320 | tf_op jit(solution)/shard_map/ppermute | solution.py:35
  85.8 6.1 %collective-permute-done.3 = bf16[512,512]{1,0:T(8,128)(2,1)S(1)} collective-permute-done((bf16[512,512]{1,0:T(8,128)(2,1)S(1)}, bf16[512,512]{1,0:T(8,128)(2,1)S(1)}, u32[]{:S(2)}, u32[]{:S(2)}) %collective-permute-start.3) | collective-permute-done | bytes 524320 | tf_op jit(solution)/shard_map/ppermute | solution.py:35
  92.2 12.1 %collective-permute-done.6 = bf16[512,512]{1,0:T(8,128)(2,1)S(1)} collective-permute-done((bf16[512,512]{1,0:T(8,128)(2,1)S(1)}, bf16[512,512]{1,0:T(8,128)(2,1)S(1)}, u32[]{:S(2)}, u32[]{:S(2)}) %collective-permute-start.6) | collective-permute-done | bytes 524320 | tf_op jit(solution)/shard_map/ppermute | solution.py:35
  105.0 9.1 %multiply_reduce_fusion.88 = (f32[4,512,8]{1,0,2:T(4,128)S(1)}, f32[4,512,8]{1,0,2:T(4,128)S(1)}, f32[4,512,8]{1,0,2:T(4,128)S(1)}, f32[4,512,8]{1,0,2:T(4,128)S...) fusion(bf16[8,4,64,512]{3,2,1,0:T(8,128)(2,1)S(1)} %bitcast.139, ...), kind=kLoop, calls=%fused_computation.172 | loop fusion | flops 58589184 | bytes 3178496
  114.6 10.4 %multiply_reduce_fusion.80 = (f32[4,512,8]{1,0,2:T(4,128)S(1)}, f32[4,512,8]{1,0,2:T(4,128)S(1)}, f32[4,512,8]{1,0,2:T(4,128)S(1)}, f32[4,512,8]{1,0,2:T(4,128)S...) fusion(bf16[8,4,64,7]{3,2,1,0:T(8,128)(2,1)S(1)} %slice.1007, ...), kind=kLoop, calls=%fused_computation.164 | loop fusion | flops 54394880 | bytes 5271552
  133.0 5.8 %multiply_reduce_fusion.78 = (f32[4,512,64]{1,2,0:T(8,128)S(1)}, f32[4,512,64]{1,2,0:T(8,128)S(1)}, f32[4,512,64]{1,2,0:T(8,128)S(1)}, f32[4,512,64]{1,2,0:T(8,1...) fusion(bf16[8,4,64,512]{3,2,1,0:T(8,128)(2,1)S(1)} %bitcast.1375, bf16[8,4,64,8]{3,2,1,0:T(8,128)(2,1)S(1)} %slice.979, ...), kind=kLoop, calls=%fused_computation.162 | loop fusion | flops 43253760 | bytes 5668864 | tf_op jit(solution)/shard_map/shc,shdc->hdc/dot_general | solution.py:113
  138.8 7.8 %multiply_reduce_fusion.70 = (f32[4,512,64]{1,2,0:T(8,128)S(1)}, f32[4,512,64]{1,2,0:T(8,128)S(1)}, f32[4,512,64]{1,2,0:T(8,128)S(1)}, f32[4,512,64]{1,2,0:T(8,1...) fusion(bf16[8,4,64,512]{3,2,1,0:T(8,128)(2,1)S(1)} %bitcast.1376, bf16[8,4,64,7]{3,2,1,0:T(8,128)(2,1)S(1)} %slice.1048, ...), kind=kLoop, calls=%fused_computation.154 | loop fusion | flops 43253760 | bytes 5664768 | tf_op jit(solution)/shard_map/shc,shdc->hdc/dot_general | solution.py:113
  155.3 26.1 %all-to-all-done.1 = bf16[8,256,512]{1,2,0:T(8,128)(2,1)S(1)} async-done(((bf16[8,256,512]{1,2,0:T(8,128)(2,1)}), bf16[8,256,512]{1,2,0:T(8,128)(2,1)S(1)}, u32[]{:S(2)}, u32[]{:S(2)}) %all-to-all-start.1) | async-done | bytes 2097184 | tf_op jit(solution)/shard_map/all_to_all | solution.py:45
  187.9 26.2 %all-to-all-done.2 = bf16[8,1,256,512]{3,2,1,0:T(8,128)(2,1)S(1)} async-done(((bf16[8,1,256,512]{3,2,1,0:T(8,128)(2,1)}), bf16[8,1,256,512]{3,2,1,0:T(8,128)(2,1)S(1)}, u32[]{:S(2)}, u32[]{:S(2)}) %all-to-all-start.2) | async-done | bytes 2097184 | tf_op jit(solution)/shard_map/all_to_all | solution.py:18
  222.2 4.5 collective-permute-start.11
  233.1 31.2 %collective-permute-done.8 = bf16[512,512]{1,0:T(8,128)(2,1)S(1)} collective-permute-done((bf16[512,512]{1,0:T(8,128)(2,1)S(1)}, bf16[512,512]{1,0:T(8,128)(2,1)S(1)}, u32[]{:S(2)}, u32[]{:S(2)}) %collective-permute-start.8) | collective-permute-done | bytes 524320 | tf_op jit(solution)/shard_map/ppermute | solution.py:35
  264.3 6.8 %collective-permute-done.10 = bf16[512,512]{1,0:T(8,128)(2,1)S(1)} collective-permute-done((bf16[512,512]{1,0:T(8,128)(2,1)S(1)}, bf16[512,512]{1,0:T(8,128)(2,1)S(1)}, u32[]{:S(2)}, u32[]{:S(2)}) %collective-permute-start.10) | collective-permute-done | bytes 524320 | tf_op jit(solution)/shard_map/ppermute | solution.py:35
  271.4 12.1 %collective-permute-done.13 = bf16[512,512]{1,0:T(8,128)(2,1)S(1)} collective-permute-done((bf16[512,512]{1,0:T(8,128)(2,1)S(1)}, bf16[512,512]{1,0:T(8,128)(2,1)S(1)}, u32[]{:S(2)}, u32[]{:S(2)}) %collective-permute-start.13) | collective-permute-done | bytes 524320 | tf_op jit(solution)/shard_map/ppermute | solution.py:35
  284.2 9.2 %multiply_reduce_fusion.56 = (f32[4,512,8]{1,0,2:T(4,128)S(1)}, f32[4,512,8]{1,0,2:T(4,128)S(1)}, f32[4,512,8]{1,0,2:T(4,128)S(1)}, f32[4,512,8]{1,0,2:T(4,128)S...) fusion(bf16[8,4,64,512]{3,2,1,0:T(8,128)(2,1)S(1)} %bitcast.139, ...), kind=kLoop, calls=%fused_computation.140 | loop fusion | flops 58589184 | bytes 3178496
  294.0 10.4 %multiply_reduce_fusion.48 = (f32[4,512,8]{1,0,2:T(4,128)S(1)}, f32[4,512,8]{1,0,2:T(4,128)S(1)}, f32[4,512,8]{1,0,2:T(4,128)S(1)}, f32[4,512,8]{1,0,2:T(4,128)S...) fusion(bf16[8,4,64,7]{3,2,1,0:T(8,128)(2,1)S(1)} %slice.1097, ...), kind=kLoop, calls=%fused_computation.132 | loop fusion | flops 54394880 | bytes 5271552
  312.4 5.8 %multiply_reduce_fusion.46 = (f32[4,512,64]{1,2,0:T(8,128)S(1)}, f32[4,512,64]{1,2,0:T(8,128)S(1)}, f32[4,512,64]{1,2,0:T(8,128)S(1)}, f32[4,512,64]{1,2,0:T(8,1...) fusion(bf16[8,4,64,512]{3,2,1,0:T(8,128)(2,1)S(1)} %bitcast.1381, bf16[8,4,64,8]{3,2,1,0:T(8,128)(2,1)S(1)} %slice.1069, ...), kind=kLoop, calls=%fused_computation.130 | loop fusion | flops 43253760 | bytes 5668864 | tf_op jit(solution)/shard_map/shc,shdc->hdc/dot_general | solution.py:113
  318.2 7.5 %multiply_reduce_fusion.38 = (f32[4,512,64]{1,2,0:T(8,128)S(1)}, f32[4,512,64]{1,2,0:T(8,128)S(1)}, f32[4,512,64]{1,2,0:T(8,128)S(1)}, f32[4,512,64]{1,2,0:T(8,1...) fusion(bf16[8,4,64,512]{3,2,1,0:T(8,128)(2,1)S(1)} %bitcast.1382, bf16[8,4,64,7]{3,2,1,0:T(8,128)(2,1)S(1)} %slice.1138, ...), kind=kLoop, calls=%fused_computation.122 | loop fusion | flops 43253760 | bytes 5664768 | tf_op jit(solution)/shard_map/shc,shdc->hdc/dot_general | solution.py:113
  328.9 29.1 %all_to_all.30 = bf16[8,256,512]{1,2,0:T(8,128)(2,1)S(1)} all-to-all(bf16[8,256,512]{1,2,0:T(8,128)(2,1)S(1)} %bitcast.1404), channel_id=1, replica_groups=mesh['sp'=32,'tp'=8] {'tp'}, dimensions={0} | all-to-all | bytes 4194304 | tf_op jit(solution)/shard_map/all_to_all | solution.py:45
  360.0 4.5 all-to-all-start.4
  364.6 26.2 %all-to-all-done.4 = bf16[8,1,256,512]{3,2,1,0:T(8,128)(2,1)S(1)} async-done(((bf16[8,1,256,512]{3,2,1,0:T(8,128)(2,1)}), bf16[8,1,256,512]{3,2,1,0:T(8,128)(2,1)S(1)}, u32[]{:S(2)}, u32[]{:S(2)}) %all-to-all-start.4) | async-done | bytes 2097184 | tf_op jit(solution)/shard_map/all_to_all | solution.py:18
  397.1 4.5 collective-permute-start.18
  408.2 31.0 %collective-permute-done.15 = bf16[512,512]{1,0:T(8,128)(2,1)S(1)} collective-permute-done((bf16[512,512]{1,0:T(8,128)(2,1)S(1)}, bf16[512,512]{1,0:T(8,128)(2,1)S(1)}, u32[]{:S(2)}, u32[]{:S(2)}) %collective-permute-start.15) | collective-permute-done | bytes 524320 | tf_op jit(solution)/shard_map/ppermute | solution.py:35
  439.2 6.7 %collective-permute-done.17 = bf16[512,512]{1,0:T(8,128)(2,1)S(1)} collective-permute-done((bf16[512,512]{1,0:T(8,128)(2,1)S(1)}, bf16[512,512]{1,0:T(8,128)(2,1)S(1)}, u32[]{:S(2)}, u32[]{:S(2)}) %collective-permute-start.17) | collective-permute-done | bytes 524320 | tf_op jit(solution)/shard_map/ppermute | solution.py:35
  446.1 12.1 %collective-permute-done.20 = bf16[512,512]{1,0:T(8,128)(2,1)S(1)} collective-permute-done((bf16[512,512]{1,0:T(8,128)(2,1)S(1)}, bf16[512,512]{1,0:T(8,128)(2,1)S(1)}, u32[]{:S(2)}, u32[]{:S(2)}) %collective-permute-start.20) | collective-permute-done | bytes 524320 | tf_op jit(solution)/shard_map/ppermute | solution.py:35
  459.0 9.5 %multiply_reduce_fusion.24 = (f32[4,512,8]{1,0,2:T(4,128)S(1)}, f32[4,512,8]{1,0,2:T(4,128)S(1)}, f32[4,512,8]{1,0,2:T(4,128)S(1)}, f32[4,512,8]{1,0,2:T(4,128)S...) fusion(bf16[8,4,64,512]{3,2,1,0:T(8,128)(2,1)S(1)} %bitcast.139, ...), kind=kLoop, calls=%fused_computation.108 | loop fusion | flops 58589184 | bytes 3178496
  469.0 10.4 %multiply_reduce_fusion.16 = (f32[4,512,8]{1,0,2:T(4,128)S(1)}, f32[4,512,8]{1,0,2:T(4,128)S(1)}, f32[4,512,8]{1,0,2:T(4,128)S(1)}, f32[4,512,8]{1,0,2:T(4,128)S...) fusion(bf16[8,4,64,7]{3,2,1,0:T(8,128)(2,1)S(1)} %slice.1187, ...), kind=kLoop, calls=%fused_computation.100 | loop fusion | flops 54394880 | bytes 5271552
  487.4 5.8 %multiply_reduce_fusion.14 = (f32[4,512,64]{1,2,0:T(8,128)S(1)}, f32[4,512,64]{1,2,0:T(8,128)S(1)}, f32[4,512,64]{1,2,0:T(8,128)S(1)}, f32[4,512,64]{1,2,0:T(8,1...) fusion(bf16[8,4,64,512]{3,2,1,0:T(8,128)(2,1)S(1)} %bitcast.1387, bf16[8,4,64,8]{3,2,1,0:T(8,128)(2,1)S(1)} %slice.1159, ...), kind=kLoop, calls=%fused_computation.98 | loop fusion | flops 43253760 | bytes 5668864 | tf_op jit(solution)/shard_map/shc,shdc->hdc/dot_general | solution.py:113
  493.1 7.5 %multiply_reduce_fusion.6 = (f32[4,512,64]{1,2,0:T(8,128)S(1)}, f32[4,512,64]{1,2,0:T(8,128)S(1)}, f32[4,512,64]{1,2,0:T(8,128)S(1)}, f32[4,512,64]{1,2,0:T(8,12...) fusion(bf16[8,4,64,512]{3,2,1,0:T(8,128)(2,1)S(1)} %bitcast.1388, bf16[8,4,64,7]{3,2,1,0:T(8,128)(2,1)S(1)} %slice.1228, ...), kind=kLoop, calls=%fused_computation.90 | loop fusion | flops 43253760 | bytes 5664768 | tf_op jit(solution)/shard_map/shc,shdc->hdc/dot_general | solution.py:113
  503.8 29.2 %all_to_all.31 = bf16[8,256,512]{1,2,0:T(8,128)(2,1)S(1)} all-to-all(bf16[8,256,512]{1,2,0:T(8,128)(2,1)S(1)} %bitcast.1406), channel_id=1, replica_groups=mesh['sp'=32,'tp'=8] {'tp'}, dimensions={0} | all-to-all | bytes 4194304 | tf_op jit(solution)/shard_map/all_to_all | solution.py:45
  (300 shorter events, 104.7 us)
Async XLA Ops:
  0.0 9.2 %copy-start.8 = (bf16[3,2048]{1,0:T(4,128)(2,1)S(1)}, bf16[3,2048]{1,0:T(4,128)(2,1)}, u32[]{:S(2)}) copy-start(bf16[3,2048]{1,0:T(4,128)(2,1)} %param.8) | copy-start | bytes 36868
  2.5 32.9 %all-to-all-start = ((bf16[8,1,256,512]{3,2,1,0:T(8,128)(2,1)}), bf16[8,1,256,512]{3,2,1,0:T(8,128)(2,1)S(1)}, u32[]{:S(2)}, u32[]{:S(2)}) async-start(bf16[8,1,256,512]{3,2,1,0:T(8,128)(2,1)} %broadcast_in_dim.9), calls=%async_computation | async-start | bytes 4194304 | tf_op jit(solution)/shard_map/all_to_all | solution.py:18
  36.5 2.3 copy-start.9
  37.9 16.2 %collective-permute-start = (bf16[512,512]{1,0:T(8,128)(2,1)S(1)}, bf16[512,512]{1,0:T(8,128)(2,1)S(1)}, u32[]{:S(2)}, u32[]{:S(2)}) collective-permute-start(bf16[512,512]{1,0:T(8,128)(2,1)S(1)} %fusion.192), channel_id=1, source_target_pairs={{224,0},{232,8},{240,16},{248,24},{0,32},{8,40},{16,48},{24,56},{3... | collective-permute-start | bytes 1572872 | tf_op jit(solution)/shard_map/ppermute | solution.py:35
  39.2 46.3 %collective-permute-start.1 = (bf16[512,512]{1,0:T(8,128)(2,1)S(1)}, bf16[512,512]{1,0:T(8,128)(2,1)S(1)}, u32[]{:S(2)}, u32[]{:S(2)}) collective-permute-start(bf16[512,512]{1,0:T(8,128)(2,1)S(1)} %fusion.192), channel_id=1, source_target_pairs={{232,0},{240,8},{248,16},{0,24},{8,32},{16,40},{24,48},{32,56},{40... | collective-permute-start | bytes 1572872 | tf_op jit(solution)/shard_map/ppermute | solution.py:35
  41.7 44.1 %collective-permute-start.2 = (bf16[512,512]{1,0:T(8,128)(2,1)S(1)}, bf16[512,512]{1,0:T(8,128)(2,1)S(1)}, u32[]{:S(2)}, u32[]{:S(2)}) collective-permute-start(bf16[512,512]{1,0:T(8,128)(2,1)S(1)} %fusion.192), channel_id=1, source_target_pairs={{240,0},{248,8},{0,16},{8,24},{16,32},{24,40},{32,48},{40,56},{48,... | collective-permute-start | bytes 1572872 | tf_op jit(solution)/shard_map/ppermute | solution.py:35
  43.6 48.4 %collective-permute-start.3 = (bf16[512,512]{1,0:T(8,128)(2,1)S(1)}, bf16[512,512]{1,0:T(8,128)(2,1)S(1)}, u32[]{:S(2)}, u32[]{:S(2)}) collective-permute-start(bf16[512,512]{1,0:T(8,128)(2,1)S(1)} %fusion.192), channel_id=1, source_target_pairs={{248,0},{0,8},{8,16},{16,24},{24,32},{32,40},{40,48},{48,56},{56,6... | collective-permute-start | bytes 1572872 | tf_op jit(solution)/shard_map/ppermute | solution.py:35
  44.2 47.9 %collective-permute-start.4 = (bf16[512,512]{1,0:T(8,128)(2,1)S(1)}, bf16[512,512]{1,0:T(8,128)(2,1)S(1)}, u32[]{:S(2)}, u32[]{:S(2)}) collective-permute-start(bf16[512,512]{1,0:T(8,128)(2,1)S(1)} %fusion.192), channel_id=1, source_target_pairs={{8,0},{16,8},{24,16},{32,24},{40,32},{48,40},{56,48},{64,56},{72,6... | collective-permute-start | bytes 1572872 | tf_op jit(solution)/shard_map/ppermute | solution.py:35
  54.1 38.0 %collective-permute-start.5 = (bf16[512,512]{1,0:T(8,128)(2,1)S(1)}, bf16[512,512]{1,0:T(8,128)(2,1)S(1)}, u32[]{:S(2)}, u32[]{:S(2)}) collective-permute-start(bf16[512,512]{1,0:T(8,128)(2,1)S(1)} %fusion.192), channel_id=1, source_target_pairs={{16,0},{24,8},{32,16},{40,24},{48,32},{56,40},{64,48},{72,56},{80,... | collective-permute-start | bytes 1572872 | tf_op jit(solution)/shard_map/ppermute | solution.py:35
  85.5 18.9 %collective-permute-start.6 = (bf16[512,512]{1,0:T(8,128)(2,1)S(1)}, bf16[512,512]{1,0:T(8,128)(2,1)S(1)}, u32[]{:S(2)}, u32[]{:S(2)}) collective-permute-start(bf16[512,512]{1,0:T(8,128)(2,1)S(1)} %fusion.192), channel_id=1, source_target_pairs={{24,0},{32,8},{40,16},{48,24},{56,32},{64,40},{72,48},{80,56},{88,... | collective-permute-start | bytes 1572872 | tf_op jit(solution)/shard_map/ppermute | solution.py:35
  149.7 5.5 %copy-start.7 = (bf16[1,256,512]{2,1,0:T(8,128)(2,1)S(1)}, bf16[1,256,512]{2,1,0:T(8,128)(2,1)}, u32[]{:S(2)}) copy-start(bf16[1,256,512]{2,1,0:T(8,128)(2,1)} %param.7) | copy-start | bytes 786436
  151.2 30.2 %all-to-all-start.1 = ((bf16[8,256,512]{1,2,0:T(8,128)(2,1)}), bf16[8,256,512]{1,2,0:T(8,128)(2,1)S(1)}, u32[]{:S(2)}, u32[]{:S(2)}) async-start(bf16[8,256,512]{1,2,0:T(8,128)(2,1)} %bitcast.1401), calls=%async_computation.1 | async-start | bytes 4194304 | tf_op jit(solution)/shard_map/all_to_all | solution.py:45
  155.3 28.1 %copy-start = (bf16[1,256,512]{1,2,0:T(8,128)(2,1)}, bf16[1,256,512]{1,2,0:T(8,128)(2,1)S(1)}, u32[]{:S(2)}) copy-start(bf16[1,256,512]{1,2,0:T(8,128)(2,1)S(1)} %copy.20) | copy-start | bytes 786436
  183.4 30.7 %all-to-all-start.2 = ((bf16[8,1,256,512]{3,2,1,0:T(8,128)(2,1)}), bf16[8,1,256,512]{3,2,1,0:T(8,128)(2,1)S(1)}, u32[]{:S(2)}, u32[]{:S(2)}) async-start(bf16[8,1,256,512]{3,2,1,0:T(8,128)(2,1)} %broadcast_in_dim.10), calls=%async_computation.2 | async-start | bytes 4194304 | tf_op jit(solution)/shard_map/all_to_all | solution.py:18
  214.1 1.5 copy-start.5
  216.9 13.8 %collective-permute-start.7 = (bf16[512,512]{1,0:T(8,128)(2,1)S(1)}, bf16[512,512]{1,0:T(8,128)(2,1)S(1)}, u32[]{:S(2)}, u32[]{:S(2)}) collective-permute-start(bf16[512,512]{1,0:T(8,128)(2,1)S(1)} %fusion.195), channel_id=1, source_target_pairs={{224,0},{232,8},{240,16},{248,24},{0,32},{8,40},{16,48},{24,56},{3... | collective-permute-start | bytes 1572872 | tf_op jit(solution)/shard_map/ppermute | solution.py:35
  220.1 44.1 %collective-permute-start.8 = (bf16[512,512]{1,0:T(8,128)(2,1)S(1)}, bf16[512,512]{1,0:T(8,128)(2,1)S(1)}, u32[]{:S(2)}, u32[]{:S(2)}) collective-permute-start(bf16[512,512]{1,0:T(8,128)(2,1)S(1)} %fusion.195), channel_id=1, source_target_pairs={{232,0},{240,8},{248,16},{0,24},{8,32},{16,40},{24,48},{32,56},{40... | collective-permute-start | bytes 1572872 | tf_op jit(solution)/shard_map/ppermute | solution.py:35
  220.2 44.1 %collective-permute-start.9 = (bf16[512,512]{1,0:T(8,128)(2,1)S(1)}, bf16[512,512]{1,0:T(8,128)(2,1)S(1)}, u32[]{:S(2)}, u32[]{:S(2)}) collective-permute-start(bf16[512,512]{1,0:T(8,128)(2,1)S(1)} %fusion.195), channel_id=1, source_target_pairs={{240,0},{248,8},{0,16},{8,24},{16,32},{24,40},{32,48},{40,56},{48,... | collective-permute-start | bytes 1572872 | tf_op jit(solution)/shard_map/ppermute | solution.py:35
  220.3 50.8 %collective-permute-start.10 = (bf16[512,512]{1,0:T(8,128)(2,1)S(1)}, bf16[512,512]{1,0:T(8,128)(2,1)S(1)}, u32[]{:S(2)}, u32[]{:S(2)}) collective-permute-start(bf16[512,512]{1,0:T(8,128)(2,1)S(1)} %fusion.195), channel_id=1, source_target_pairs={{248,0},{0,8},{8,16},{16,24},{24,32},{32,40},{40,48},{48,56},{56,6... | collective-permute-start | bytes 1572872 | tf_op jit(solution)/shard_map/ppermute | solution.py:35
  222.2 49.1 %collective-permute-start.11 = (bf16[512,512]{1,0:T(8,128)(2,1)S(1)}, bf16[512,512]{1,0:T(8,128)(2,1)S(1)}, u32[]{:S(2)}, u32[]{:S(2)}) collective-permute-start(bf16[512,512]{1,0:T(8,128)(2,1)S(1)} %fusion.195), channel_id=1, source_target_pairs={{8,0},{16,8},{24,16},{32,24},{40,32},{48,40},{56,48},{64,56},{72,6... | collective-permute-start | bytes 1572872 | tf_op jit(solution)/shard_map/ppermute | solution.py:35
  230.7 40.6 %collective-permute-start.12 = (bf16[512,512]{1,0:T(8,128)(2,1)S(1)}, bf16[512,512]{1,0:T(8,128)(2,1)S(1)}, u32[]{:S(2)}, u32[]{:S(2)}) collective-permute-start(bf16[512,512]{1,0:T(8,128)(2,1)S(1)} %fusion.195), channel_id=1, source_target_pairs={{16,0},{24,8},{32,16},{40,24},{48,32},{56,40},{64,48},{72,56},{80,... | collective-permute-start | bytes 1572872 | tf_op jit(solution)/shard_map/ppermute | solution.py:35
  264.3 19.2 %collective-permute-start.13 = (bf16[512,512]{1,0:T(8,128)(2,1)S(1)}, bf16[512,512]{1,0:T(8,128)(2,1)S(1)}, u32[]{:S(2)}, u32[]{:S(2)}) collective-permute-start(bf16[512,512]{1,0:T(8,128)(2,1)S(1)} %fusion.195), channel_id=1, source_target_pairs={{24,0},{32,8},{40,16},{48,24},{56,32},{64,40},{72,48},{80,56},{88,... | collective-permute-start | bytes 1572872 | tf_op jit(solution)/shard_map/ppermute | solution.py:35
  360.0 30.8 %all-to-all-start.4 = ((bf16[8,1,256,512]{3,2,1,0:T(8,128)(2,1)}), bf16[8,1,256,512]{3,2,1,0:T(8,128)(2,1)S(1)}, u32[]{:S(2)}, u32[]{:S(2)}) async-start(bf16[8,1,256,512]{3,2,1,0:T(8,128)(2,1)} %broadcast_in_dim.11), calls=%async_computation.4 | async-start | bytes 4194304 | tf_op jit(solution)/shard_map/all_to_all | solution.py:18
  390.8 1.5 copy-start.3
  393.6 13.8 %collective-permute-start.14 = (bf16[512,512]{1,0:T(8,128)(2,1)S(1)}, bf16[512,512]{1,0:T(8,128)(2,1)S(1)}, u32[]{:S(2)}, u32[]{:S(2)}) collective-permute-start(bf16[512,512]{1,0:T(8,128)(2,1)S(1)} %fusion.198), channel_id=1, source_target_pairs={{224,0},{232,8},{240,16},{248,24},{0,32},{8,40},{16,48},{24,56},{3... | collective-permute-start | bytes 1572872 | tf_op jit(solution)/shard_map/ppermute | solution.py:35
  395.1 44.1 %collective-permute-start.15 = (bf16[512,512]{1,0:T(8,128)(2,1)S(1)}, bf16[512,512]{1,0:T(8,128)(2,1)S(1)}, u32[]{:S(2)}, u32[]{:S(2)}) collective-permute-start(bf16[512,512]{1,0:T(8,128)(2,1)S(1)} %fusion.198), channel_id=1, source_target_pairs={{232,0},{240,8},{248,16},{0,24},{8,32},{16,40},{24,48},{32,56},{40... | collective-permute-start | bytes 1572872 | tf_op jit(solution)/shard_map/ppermute | solution.py:35
  395.1 44.1 %collective-permute-start.16 = (bf16[512,512]{1,0:T(8,128)(2,1)S(1)}, bf16[512,512]{1,0:T(8,128)(2,1)S(1)}, u32[]{:S(2)}, u32[]{:S(2)}) collective-permute-start(bf16[512,512]{1,0:T(8,128)(2,1)S(1)} %fusion.198), channel_id=1, source_target_pairs={{240,0},{248,8},{0,16},{8,24},{16,32},{24,40},{32,48},{40,56},{48,... | collective-permute-start | bytes 1572872 | tf_op jit(solution)/shard_map/ppermute | solution.py:35
  395.2 50.7 %collective-permute-start.17 = (bf16[512,512]{1,0:T(8,128)(2,1)S(1)}, bf16[512,512]{1,0:T(8,128)(2,1)S(1)}, u32[]{:S(2)}, u32[]{:S(2)}) collective-permute-start(bf16[512,512]{1,0:T(8,128)(2,1)S(1)} %fusion.198), channel_id=1, source_target_pairs={{248,0},{0,8},{8,16},{16,24},{24,32},{32,40},{40,48},{48,56},{56,6... | collective-permute-start | bytes 1572872 | tf_op jit(solution)/shard_map/ppermute | solution.py:35
  397.1 48.9 %collective-permute-start.18 = (bf16[512,512]{1,0:T(8,128)(2,1)S(1)}, bf16[512,512]{1,0:T(8,128)(2,1)S(1)}, u32[]{:S(2)}, u32[]{:S(2)}) collective-permute-start(bf16[512,512]{1,0:T(8,128)(2,1)S(1)} %fusion.198), channel_id=1, source_target_pairs={{8,0},{16,8},{24,16},{32,24},{40,32},{48,40},{56,48},{64,56},{72,6... | collective-permute-start | bytes 1572872 | tf_op jit(solution)/shard_map/ppermute | solution.py:35
  407.4 38.6 %collective-permute-start.19 = (bf16[512,512]{1,0:T(8,128)(2,1)S(1)}, bf16[512,512]{1,0:T(8,128)(2,1)S(1)}, u32[]{:S(2)}, u32[]{:S(2)}) collective-permute-start(bf16[512,512]{1,0:T(8,128)(2,1)S(1)} %fusion.198), channel_id=1, source_target_pairs={{16,0},{24,8},{32,16},{40,24},{48,32},{56,40},{64,48},{72,56},{80,... | collective-permute-start | bytes 1572872 | tf_op jit(solution)/shard_map/ppermute | solution.py:35
  439.2 19.1 %collective-permute-start.20 = (bf16[512,512]{1,0:T(8,128)(2,1)S(1)}, bf16[512,512]{1,0:T(8,128)(2,1)S(1)}, u32[]{:S(2)}, u32[]{:S(2)}) collective-permute-start(bf16[512,512]{1,0:T(8,128)(2,1)S(1)} %fusion.198), channel_id=1, source_target_pairs={{24,0},{32,8},{40,16},{48,24},{56,32},{64,40},{72,48},{80,56},{88,... | collective-permute-start | bytes 1572872 | tf_op jit(solution)/shard_map/ppermute | solution.py:35
  503.8 29.6 %copy-start.1 = (bf16[1,256,512]{1,2,0:T(8,128)(2,1)S(1)}, bf16[1,256,512]{1,2,0:T(8,128)(2,1)}, u32[]{:S(2)}) copy-start(bf16[1,256,512]{1,2,0:T(8,128)(2,1)} %copy-done) | copy-start | bytes 786436
  (3 other events, 3.7 us)
where the time goes:
time: 542 us; the launch traced here: 535 us
  waiting for transfers between devices  255 us (47%)
  other arithmetic  129 us (24%)
  blocking collectives  58.3 us (11%)
  starting transfers between devices  53.9 us (10%)
  local copies, waits for them, and re-layouts  21.6 us (4%)
  matrix products  15.6 us (3%)
    ppermute x21, waiting for transfers between devices, from_behind(): return lax.ppermute(block, axis, route)  156 us
    all_to_all x3, waiting for transfers between devices, copy_for_each(): lax.all_to_all(jnp.broadcast_to(x[None], (size, *x.shape)), axis, 0, 0, t...  73.4 us
    unnamed x54, other arithmetic  62.8 us
    all_to_all x2, blocking collectives, sent_and_summed(): lax.all_to_all(pieces, axis, split_axis=0, concat_axis=0, tiled=True)  58.3 us
    dot_general x12, other arithmetic, body(): jnp.einsum('shc,shdc->hdc', weights[offset], shifted, preferred_element_t...  52.2 us
    ppermute x21, starting transfers between devices, from_behind(): return lax.ppermute(block, axis, route)  34.2 us
    all_to_all x1, waiting for transfers between devices, sent_and_summed(): lax.all_to_all(pieces, axis, split_axis=0, concat_axis=0, tiled=True)  26.1 us
    all_to_all x3, starting transfers between devices, copy_for_each(): lax.all_to_all(jnp.broadcast_to(x[None], (size, *x.shape)), axis, 0, 0, t...  15.7 us
  transfers between devices with their start and end apart: 25, of which 16 were waited for; matrix products, arithmetic and copies ran while one was open for 2% of the time, Pallas kernels for 0%

commit v1 on v0

v1 whole, which is shorter than its diff:
```python
import functools

import jax
import jax.numpy as jnp
from jax import lax
from jax.experimental import pallas as pl
from jax.experimental.pallas import tpu as pltpu
from jax.sharding import PartitionSpec as P

D = 2048
HEADS_DEV = 4
HEAD_DIM = 64
CH = 256
N_TP = 8
WIN_R = 8
WIN_C = 16
LAYERS = 3
ROWS = 32
BLOCK_C = 16
STRIP_C = 8
STRIP = ROWS * STRIP_C
HALF = STRIP // 2
TILE_Q = 64
TILES = STRIP // TILE_Q
EPS = 1e-06
NEG = -1e30
MESH = pl.DeviceIdType.MESH
F32 = jnp.float32
BF16 = jnp.bfloat16


def dot(a, b):
    return lax.dot_general(a, b, (((1,), (0,)), ((), ())), preferred_element_type=F32)


def dot_nt(a, b):
    return lax.dot_general(a, b, (((1,), (1,)), ((), ())), preferred_element_type=F32)


def kernel(
    n_sp, x_ref, gain_ref, base_ref, wq_ref, wk_ref, wv_ref, wo_ref, out_ref,
    wqkv, wout, xg, acc, sq, qs_ref, kv, bias, mixed, part, ssum, own, pd2d, rs_y,
    w_sem, ag_s, ag_r, d_s, d_r, y_s, y_r, h_s, h_r,
):
    tp = lax.axis_index("tp")
    sp = lax.axis_index("sp")
    y, core = tp // 2, tp % 2
    right = ((y + 1) % 4) * 2 + core
    left = ((y + 3) % 4) * 2 + core
    opp = ((y + 2) % 4) * 2 + core
    partner = y * 2 + 1 - core
    flip = 1 - 2 * core
    after = (sp + 1) % n_sp
    before = (sp + n_sp - 1) % n_sp

    barrier = pltpu.get_barrier_semaphore()
    for target in ({"tp": right}, {"tp": left}, {"tp": partner}, {"sp": after}, {"sp": before}):
        pl.semaphore_signal(barrier, inc=1, device_id=target, device_id_type=MESH)

    def weight_copies(l):
        copies = []
        for i, ref in enumerate((wq_ref, wk_ref, wv_ref)):
            copies.append(
                pltpu.make_async_copy(ref.at[l], wqkv.at[l, :, :, pl.ds(i * CH, CH)], w_sem.at[l, i])
            )
        for b in range(N_TP):
            copies.append(
                pltpu.make_async_copy(
                    wo_ref.at[l, :, pl.ds(b * CH, CH)], wout.at[l, b], w_sem.at[l, 3 + b]
                )
            )
        return copies

    for l in range(LAYERS):
        for copy in weight_copies(l):
            copy.start()
    for s in range(2):
        xg[s, tp] = x_ref[s]

    def remote(src, dst, s_sem, r_sem, target):
        return pltpu.make_async_remote_copy(
            src_ref=src, dst_ref=dst, send_sem=s_sem, recv_sem=r_sem,
            device_id=target, device_id_type=MESH,
        )

    first, second = pl.ds(0, HALF), pl.ds(HALF, HALF)
    whole = pl.ds(0, STRIP)
    gather = (
        (tp, first, right), (tp, second, right), (left, first, right),
        (tp, second, left), (tp, first, left), (right, second, left),
        (tp, whole, partner), (left, first, partner), (left, second, partner),
        (right, first, partner), (right, second, partner),
        (opp, first, partner), (opp, second, partner),
    )

    def ag(s, k):
        owner, span, target = gather[k]
        ref = xg.at[s, owner, span]
        return remote(ref, ref, ag_s.at[s, k], ag_r.at[s, k], {"tp": target})

    sides = (opp, right, left, tp)

    def die(s, k):
        return remote(part.at[s, k], pd2d.at[s, k], d_s.at[s, k], d_r.at[s, k], {"tp": partner})

    scatter = (
        (0, first, right), (0, second, left), (1, second, right),
        (2, first, left), (1, first, right), (2, second, left),
    )

    def ring(s, k):
        side, span, target = scatter[k]
        return remote(ssum.at[s, side, span], rs_y.at[s, k], y_s.at[s, k], y_r.at[s, k], {"tp": target})

    def halo(s, par):
        return remote(
            kv.at[par, 1 + s], kv.at[par, 3 * (1 - s)], h_s.at[par, s], h_r.at[par, s],
            {"sp": (sp + 2 * s - 1 + n_sp) % n_sp},
        )

    lane_head = lax.broadcasted_iota(jnp.int32, (TILE_Q, CH), 1) // HEAD_DIM
    head_mask = [(lane_head == h).astype(F32).astype(BF16) for h in range(HEADS_DEV)]

    def start_own(s):
        for k in (0, 3, 6, 1, 4):
            ag(s, k).start()

    def arrive(s, k, *onward):
        ag(s, k).wait_recv()
        for j in onward:
            ag(s, j).start()

    def accumulate(s, l, blocks, fresh):
        total = None
        squares = None
        for b in blocks:
            xb = xg[s, b]
            wide = xb.astype(F32)
            sq_b = wide * wide
            sq_b = sq_b[:, :128] + sq_b[:, 128:]
            squares = sq_b if squares is None else squares + sq_b
            scaled = (wide * gain_ref[l, b]).astype(BF16)
            term = dot(scaled, wqkv[l, b])
            total = term if total is None else total + term
        if fresh:
            acc[...] = total
            sq[...] = squares
        else:
            acc[...] += total
            sq[...] += squares

    def project(s, l, par, mid):
        arrive(s, 0, 2, 7)
        arrive(s, 3, 5, 10)
        mid()
        arrive(s, 6)
        accumulate(s, l, (tp, partner), True)
        arrive(s, 1, 8)
        arrive(s, 4, 9)
        accumulate(s, l, (left, right), False)
        for k in (7, 8, 9, 10):
            arrive(s, k)
        accumulate(s, l, (left + flip, right + flip), False)
        arrive(s, 2, 11)
        arrive(s, 5, 12)
        arrive(s, 11)
        arrive(s, 12)
        accumulate(s, l, (opp, opp + flip), False)
        inverse = lax.rsqrt(jnp.sum(sq[...], axis=1, keepdims=True) / D + EPS)
        kv[par, 1 + s] = (acc[:, CH:] * inverse).astype(BF16)
        halo(s, par).start()
        qs_ref[s] = (acc[:, :CH] * (inverse * HEAD_DIM**-0.5)).astype(BF16)
        for k in range(13):
            ag(s, k).wait_send()

    def window(par, slot, t, lo, hi):
        start = t * TILE_Q - 4 * STRIP_C
        stop = start + 16 * STRIP_C
        if start < 0:
            return jnp.concatenate(
                [kv[par, slot, STRIP + start:, lo:hi], kv[par, slot, :stop, lo:hi]], axis=0
            )
        if stop > STRIP:
            return jnp.concatenate(
                [kv[par, slot, start:, lo:hi], kv[par, slot, : stop - STRIP, lo:hi]], axis=0
            )
        return kv[par, slot, start:stop, lo:hi]

    def attend(s, l, par):
        for t in range(TILES):
            q = qs_ref[s, t * TILE_Q : (t + 1) * TILE_Q, :]
            q_all = jnp.concatenate([q * m for m in head_mask], axis=0)
            table = bias[pl.ds(HEADS_DEV * l, HEADS_DEV)].reshape(HEADS_DEV * TILE_Q, 3 * 128)
            scores = jnp.concatenate(
                [dot_nt(q_all, window(par, s + j, t, 0, CH)) for j in range(3)], axis=1
            ) + table
            highest = jnp.max(scores, axis=1, keepdims=True)
            weights = jnp.exp(scores - highest)
            total = jnp.sum(weights, axis=1, keepdims=True)
            weights = weights.astype(BF16)
            values = jnp.concatenate(
                [window(par, s + j, t, CH, 2 * CH) for j in range(3)], axis=0
            )
            o = dot(weights, values) / total
            out = o[:TILE_Q]
            for h in range(1, HEADS_DEV):
                out = jnp.where(lane_head == h, o[h * TILE_Q : (h + 1) * TILE_Q], out)
            mixed[s, t * TILE_Q : (t + 1) * TILE_Q, :] = out.astype(BF16)

    def send_partner(s, l):
        for k in range(4):
            part[s, k] = dot(mixed[s], wout[l, sides[k] + flip]).astype(BF16)
            die(s, k).start()

    def pair(s, l, k):
        mine = dot(mixed[s], wout[l, sides[k]])
        die(s, k).wait_recv()
        return mine + pd2d[s, k].astype(F32)

    def ring_first(s, l):
        ssum[s, 0] = pair(s, l, 0).astype(BF16)
        ring(s, 0).start()
        ring(s, 1).start()
        ssum[s, 1] = pair(s, l, 1).astype(BF16)
        ring(s, 2).start()
        ssum[s, 2] = pair(s, l, 2).astype(BF16)
        ring(s, 3).start()
        own[s] = pair(s, l, 3) + xg[s, tp].astype(F32)

    def ring_relay(s):
        for k, span in ((0, first), (1, second)):
            ring(s, k).wait_recv()
            side = 1 + k
            ssum[s, side, span] = (
                ssum[s, side, span].astype(F32) + rs_y[s, k].astype(F32)
            ).astype(BF16)
            ring(s, 4 + k).start()

    def ring_last(s):
        for k in (2, 3, 4, 5):
            ring(s, k).wait_recv()
        xg[s, tp, first] = (
            own[s, first] + rs_y[s, 4].astype(F32) + rs_y[s, 3].astype(F32)
        ).astype(BF16)
        xg[s, tp, second] = (
            own[s, second] + rs_y[s, 2].astype(F32) + rs_y[s, 5].astype(F32)
        ).astype(BF16)
        for k in range(4):
            die(s, k).wait_send()
        for k in range(6):
            ring(s, k).wait_send()

    pl.semaphore_wait(barrier, 5)
    start_own(0)

    lane_c = lax.broadcasted_iota(jnp.int32, (8, 128), 1) % STRIP_C
    row_c = lax.broadcasted_iota(jnp.int32, (8, 128), 0)
    nothing = jnp.full((8, 128), NEG, F32)

    def build(i, carry):
        lanes = [jnp.broadcast_to(base_ref[i, pl.ds(j, 1)], (8, 128)) for j in range(2)]
        straight = [pltpu.roll(g, 0, 1, stride=1, stride_axis=0) for g in lanes] + [nothing]
        carried = [nothing] + [pltpu.roll(g, 128 - STRIP_C, 1, stride=1, stride_axis=0) for g in lanes]
        for j in range(3):
            t = jnp.where(lane_c >= row_c, straight[j], carried[j])
            for r in range(8):
                bias[i, r * 8 : (r + 1) * 8, j * 128 : (j + 1) * 128] = (
                    t if r == 0 else pltpu.roll(t, r * STRIP_C, 1)
                )
        return carry

    lax.fori_loop(0, LAYERS * HEADS_DEV, build, 0)

    def layer(l, carry):
        par = l % 2
        f, g = par, 1 - par
        for copy in weight_copies(l):
            copy.wait()
        project(f, l, par, lambda: start_own(g))
        project(g, l, par, lambda: None)
        halo(f, par).wait_recv()
        attend(g, l, par)
        send_partner(g, l)
        halo(g, par).wait_recv()
        attend(f, l, par)
        ring_first(g, l)
        send_partner(f, l)
        ring_relay(g)
        ring_first(f, l)
        ring_last(g)

        @pl.when(l < LAYERS - 1)
        def _():
            start_own(g)

        ring_relay(f)
        ring_last(f)
        halo(f, par).wait_send()
        halo(g, par).wait_send()
        return carry

    lax.fori_loop(0, LAYERS, layer, 0)
    for s in range(2):
        out_ref[s] = xg[s, tp]


def run_layers(n_sp, x, gain, base, wq, wk, wv, wo):
    vmem = pl.BlockSpec(memory_space=pltpu.VMEM)
    hbm = pl.BlockSpec(memory_space=pl.ANY)
    dma = pltpu.SemaphoreType.DMA
    return pl.pallas_call(
        functools.partial(kernel, n_sp),
        out_shape=jax.ShapeDtypeStruct((2, STRIP, CH), BF16),
        in_specs=[vmem, vmem, vmem, hbm, hbm, hbm, hbm],
        out_specs=vmem,
        scratch_shapes=[
            pltpu.VMEM((LAYERS, N_TP, CH, 3 * CH), BF16),
            pltpu.VMEM((LAYERS, N_TP, CH, CH), BF16),
            pltpu.VMEM((2, N_TP, STRIP, CH), BF16),
            pltpu.VMEM((STRIP, 3 * CH), F32),
            pltpu.VMEM((STRIP, 128), F32),
            pltpu.VMEM((2, STRIP, CH), BF16),
            pltpu.VMEM((2, 4, STRIP, 2 * CH), BF16),
            pltpu.VMEM((LAYERS * HEADS_DEV, TILE_Q, 3 * 128), F32),
            pltpu.VMEM((2, STRIP, CH), BF16),
            pltpu.VMEM((2, 4, STRIP, CH), BF16),
            pltpu.VMEM((2, 3, STRIP, CH), BF16),
            pltpu.VMEM((2, STRIP, CH), F32),
            pltpu.VMEM((2, 4, STRIP, CH), BF16),
            pltpu.VMEM((2, 6, HALF, CH), BF16),
            dma((LAYERS, 3 + N_TP)), dma((2, 13)), dma((2, 13)), dma((2, 4)), dma((2, 4)),
            dma((2, 6)), dma((2, 6)), dma((2, 2)), dma((2, 2)),
        ],
        compiler_params=pltpu.CompilerParams(
            collective_id=0, has_side_effects=True, vmem_limit_bytes=60 * 1024 * 1024
        ),
    )(x, gain, base, wq, wk, wv, wo)


def body(token_grid, norm_gain, w_query, w_key, w_value, w_out, rel_bias):
    n_sp = lax.axis_size("sp")
    rows = token_grid.shape[0]
    gain = norm_gain.astype(F32).reshape(LAYERS, N_TP, 1, CH)
    base = rel_bias.reshape(LAYERS * HEADS_DEV, WIN_R, 2, STRIP_C).transpose(0, 2, 1, 3)
    base = base.reshape(LAYERS * HEADS_DEV, 2, WIN_R * STRIP_C)
    base = jnp.pad(base, ((0, 0), (0, 0), (0, 64)), constant_values=NEG)
    wq, wk, wv = (w.reshape(LAYERS, N_TP, CH, CH) for w in (w_query, w_key, w_value))

    x = token_grid.reshape(rows, CH, n_sp, BLOCK_C).transpose(2, 0, 3, 1)
    x = lax.all_to_all(x, "sp", 0, 0, tiled=True)
    x = x.reshape(ROWS, 2, STRIP_C, CH).transpose(1, 0, 2, 3).reshape(2, STRIP, CH)
    x = run_layers(n_sp, x, gain, base, wq, wk, wv, w_out)
    x = x.reshape(2, ROWS, STRIP_C, CH).transpose(1, 0, 2, 3)
    x = x.reshape(n_sp, rows, BLOCK_C, CH)
    x = lax.all_to_all(x, "sp", 0, 0, tiled=True)
    return x.transpose(1, 3, 0, 2).reshape(rows, CH, n_sp * BLOCK_C)


def solution(mesh):
    in_specs = (
        P("sp", "tp", None),
        P(),
        P(None, None, "tp"),
        P(None, None, "tp"),
        P(None, None, "tp"),
        P(None, "tp", None),
        P(None, "tp", None, None),
    )
    out_specs = P("sp", "tp", None)
    return jax.shard_map(body, mesh=mesh, in_specs=in_specs, out_specs=out_specs, check_vma=False)
```

time: 542 us -> 161 us (0.30)
  waiting for transfers between devices: 255 us -> 8.31 us
  other arithmetic: 129 us -> 0 us
  Pallas kernels: 0 us -> 118 us
  blocking collectives: 58.3 us -> 13.4 us
  starting transfers between devices: 53.9 us -> 11.9 us
  matrix products: 15.6 us -> 0 us
  local copies, waits for them, and re-layouts: 21.6 us -> 7.3 us
    ppermute x21 -> x0, waiting for transfers between devices: 156 us -> none  [from_behind(): return lax.ppermute(block, axis, route)]
    pallas_call x0 -> x1, Pallas kernels: none -> 118 us  [run_layers(): pl.pallas_call(functools.partial(kernel, n_sp), out_shape=jax.ShapeDtypeS...]
    all_to_all x4 -> x1, waiting for transfers between devices: 99.5 us -> 8.31 us  [body(): x = lax.all_to_all(x, 'sp', 0, 0, tiled=True)]
    unnamed x54 -> x0, other arithmetic: 62.8 us -> none
    dot_general x12 -> x0, other arithmetic: 52.2 us -> none  [body(): jnp.einsum('shc,shdc->hdc', weights[offset], shifted, preferred_element_t...]
    all_to_all x2 -> x1, blocking collectives: 58.3 us -> 13.4 us  [body(): x = lax.all_to_all(x, 'sp', 0, 0, tiled=True)]
    ppermute x21 -> x0, starting transfers between devices: 34.2 us -> none  [from_behind(): return lax.ppermute(block, axis, route)]
    dot_general x9 -> x0, matrix products: 15.6 us -> none  [the longest x3 5.96 us: body(): lax.dot_general(rows_query, scaled, contract, preferred_element_type=jnp....]
  transfers between devices with their start and end apart: 25 -> 1, of which waited for: 16 -> 1; matrix products, arithmetic and copies ran while one was open for 2% -> 2% of each run, Pallas kernels for 0% -> 0%
where the time goes in v1:
time: 161 us; the launch traced here: 158 us
  Pallas kernels  118 us (73%)
  blocking collectives  13.4 us (8%)
  starting transfers between devices  11.9 us (7%)
  waiting for transfers between devices  8.31 us (5%)
  local copies, waits for them, and re-layouts  7.3 us (5%)
    pallas_call x1, Pallas kernels, run_layers(): pl.pallas_call(functools.partial(kernel, n_sp), out_shape=jax.ShapeDtypeS...  118 us
    all_to_all x1, blocking collectives, body(): x = lax.all_to_all(x, 'sp', 0, 0, tiled=True)  13.4 us
    all_to_all x1, starting transfers between devices, body(): x = lax.all_to_all(x, 'sp', 0, 0, tiled=True)  11.9 us
    all_to_all x1, waiting for transfers between devices, body(): x = lax.all_to_all(x, 'sp', 0, 0, tiled=True)  8.31 us
  transfers between devices with their start and end apart: 1, of which 1 were waited for; matrix products, arithmetic and copies ran while one was open for 2% of the time, Pallas kernels for 0%

profile of v1, /device:TPU:1, one launch (start us, length us, event | category | flops | bytes accessed | tf_op | source)
XLA Modules:
  0.0 158.5 jit_solution(5306670498093502322)
XLA Ops:
  0.0 1.8 %copy.14 = bf16[1,256,512]{1,2,0:T(8,128)(2,1)} copy(bf16[1,256,512]{2,1,0:T(8,128)(2,1)} %param.7) | data formatting | bytes 524288 | tf_op args[0]
  1.8 11.9 %all-to-all-start = ((bf16[32,1,16,256]{3,2,1,0:T(8,128)(2,1)}), bf16[32,1,16,256]{3,2,1,0:T(8,128)(2,1)S(1)}, u32[]{:S(2)}, u32[]{:S(2)}) async-start(bf16[32,1,16,256]{3,2,1,0:T(8,128)(2,1)} %bitcast.2), calls=%async_computation | async-start | bytes 524288 | tf_op jit(solution)/shard_map/all_to_all | solution.py:350
  13.7 0.9 reshape.43
  14.6 0.1 reshape.44
  14.7 1.4 reshape.52.gain_ref
  16.1 0.6 pad.4.base_ref
  16.7 8.3 %all-to-all-done = bf16[32,1,16,256]{3,2,1,0:T(8,128)(2,1)S(1)} async-done(((bf16[32,1,16,256]{3,2,1,0:T(8,128)(2,1)}), bf16[32,1,16,256]{3,2,1,0:T(8,128)(2,1)S(1)}, u32[]{:S(2)}, u32[]{:S(2)}) %all-to-all-start) | async-done | bytes 262176 | tf_op jit(solution)/shard_map/all_to_all | solution.py:350
  25.0 0.7 copy_bitcast_fusion.1.x_ref
  25.7 117.6 %shard_map.73 = bf16[2,256,256]{2,1,0:T(8,128)(2,1)} custom-call(bf16[2,256,256]{2,1,0:T(8,128)(2,1)} %copy_bitcast_fusion.1.x_ref, f32[3,8,1,256]{3,2,1,0:T(1,128)} %reshape.52.gain_ref, f32[12,2,128]{2,1,0:T(2,128)} %pad.4.base_ref, bf16[3,8,256,256]{3,2,1,0:T(8,128)(2,1)} %bitcast.34, bf16[3,8,256,256]{3,2,1,0:T(8,128)(2,1)} %bitcast.35, ...), custom_call_target="tpu_custom_call" | custom-call | tf_op jit(solution)/shard_map/pallas_call | solution.py:311
  143.3 1.0 copy_bitcast_fusion
  144.2 13.4 %all_to_all.10 = bf16[32,1,16,256]{3,2,1,0:T(8,128)(2,1)S(1)} all-to-all(bf16[32,1,16,256]{3,2,1,0:T(8,128)(2,1)S(1)} %copy_bitcast_fusion), channel_id=1, replica_groups=mesh['sp'=32,'tp'=8] {'sp'}, dimensions={0} | all-to-all | bytes 524288 | tf_op jit(solution)/shard_map/all_to_all | solution.py:355
  157.6 0.8 copy.21
  (1 shorter events, 0.0 us)
Async XLA Ops:
  1.8 23.2 %all-to-all-start = ((bf16[32,1,16,256]{3,2,1,0:T(8,128)(2,1)}), bf16[32,1,16,256]{3,2,1,0:T(8,128)(2,1)S(1)}, u32[]{:S(2)}, u32[]{:S(2)}) async-start(bf16[32,1,16,256]{3,2,1,0:T(8,128)(2,1)} %bitcast.2), calls=%async_computation | async-start | bytes 524288 | tf_op jit(solution)/shard_map/all_to_all | solution.py:350

commit v2 on v0

v2 whole, which is shorter than its diff:
```python
import functools

import jax
import jax.numpy as jnp
from jax import lax
from jax.experimental import pallas as pl
from jax.experimental.pallas import tpu as pltpu
from jax.sharding import PartitionSpec as P

D = 2048
HEADS_DEV = 4
HEAD_DIM = 64
CH = 256
N_TP = 8
WIN_R = 8
WIN_C = 16
LAYERS = 3
ROWS = 32
GROUPS = 4
STRIP_C = 8
TILE = 64
TOK = 2 * TILE
EPS = 1e-06
NEG = -1e30
MESH = pl.DeviceIdType.MESH
F32 = jnp.float32
BF16 = jnp.bfloat16


def dot(a, b):
    return lax.dot_general(a, b, (((1,), (0,)), ((), ())), preferred_element_type=F32)


def dot_nt(a, b):
    return lax.dot_general(a, b, (((1,), (1,)), ((), ())), preferred_element_type=F32)


def kernel(
    n_sp, rows, x_ref, gain_ref, bias_ref, wq_ref, wk_ref, wv_ref, wo_ref, out_ref,
    x_src, x_dst, o_src, o_dst,
    wqkv, wout, gains, pad, bias, xg, acc, sq, qs, kv, mixed, part, ssum, own, pd2d, rs_y,
    w_sem, x_s, x_r, o_s, o_r, ag_s, ag_r, d_s, d_r, y_s, y_r, h_s, h_r,
):
    tp = lax.axis_index("tp")
    sp = lax.axis_index("sp")
    y, core = tp // 2, tp % 2
    right = ((y + 1) % 4) * 2 + core
    left = ((y + 3) % 4) * 2 + core
    opp = ((y + 2) % 4) * 2 + core
    partner = y * 2 + 1 - core
    flip = 1 - 2 * core

    barrier = pltpu.get_barrier_semaphore()
    for target in (right, left, partner):
        pl.semaphore_signal(barrier, inc=1, device_id={"tp": target}, device_id_type=MESH)

    def greet(i, carry):
        pl.semaphore_signal(
            barrier, inc=1, device_id={"sp": (sp + i) % n_sp}, device_id_type=MESH
        )
        return carry

    lax.fori_loop(1, n_sp, greet, 0)

    def weight_copies(l):
        copies = []
        for i, ref in enumerate((wq_ref, wk_ref, wv_ref)):
            copies.append(
                pltpu.make_async_copy(ref.at[l], wqkv.at[l, :, :, pl.ds(i * CH, CH)], w_sem.at[l, i])
            )
        for b in range(N_TP):
            copies.append(
                pltpu.make_async_copy(
                    wo_ref.at[l, :, pl.ds(b * CH, CH)], wout.at[l, b], w_sem.at[l, 3 + b]
                )
            )
        return copies

    for l in range(LAYERS):
        for copy in weight_copies(l):
            copy.start()

    def remote(src, dst, s_sem, r_sem, target):
        return pltpu.make_async_remote_copy(
            src_ref=src, dst_ref=dst, send_sem=s_sem, recv_sem=r_sem,
            device_id=target, device_id_type=MESH,
        )

    for r in range(rows):
        turned = x_ref[r].astype(F32).T
        x_src[:, r] = turned.reshape(n_sp, 2, STRIP_C, CH).astype(BF16)

    def scatter_in(i, carry):
        target = (sp + i) % n_sp
        remote(
            x_src.at[target], x_dst.at[pl.ds(sp * rows, rows)], x_s.at[0], x_r.at[0], {"sp": target}
        ).start()
        return carry

    pl.semaphore_wait(barrier, n_sp + 2)
    lax.fori_loop(1, n_sp, scatter_in, 0)
    x_dst[pl.ds(sp * rows, rows)] = x_src[sp]

    for l in range(LAYERS):
        for b in range(N_TP):
            gains[l, b] = gain_ref[l : l + 1, b * CH : (b + 1) * CH].astype(F32)
    pad[...] = jnp.zeros_like(pad)
    for i in range(LAYERS * HEADS_DEV):
        pad[i, :, :WIN_C] = bias_ref[i // HEADS_DEV, i % HEADS_DEV]
    lane = lax.broadcasted_iota(jnp.int32, (8, 128), 1)
    lane_c = lane % STRIP_C
    row_c = lax.broadcasted_iota(jnp.int32, (8, 128), 0)
    nothing = jnp.full((8, 128), NEG, F32)

    def build(i, carry):
        table = pad[i]
        lanes = []
        for j in range(2):
            piece = table if j == 0 else pltpu.roll(table, 128 - STRIP_C, 1)
            piece = jnp.where(lane < STRIP_C, piece, 0.0)
            piece = pltpu.roll(piece, 0, 1, stride=STRIP_C, stride_axis=0)
            piece = jnp.broadcast_to(jnp.sum(piece, axis=0, keepdims=True), (8, 128))
            lanes.append(jnp.where(lane < WIN_R * STRIP_C, piece, NEG))
        straight = [pltpu.roll(g, 0, 1, stride=1, stride_axis=0) for g in lanes] + [nothing]
        carried = [nothing] + [pltpu.roll(g, 128 - STRIP_C, 1, stride=1, stride_axis=0) for g in lanes]
        for j in range(3):
            t = jnp.where(lane_c >= row_c, straight[j], carried[j])
            for r in range(8):
                bias[i, r * 8 : (r + 1) * 8, j * 128 : (j + 1) * 128] = (
                    t if r == 0 else pltpu.roll(t, r * STRIP_C, 1)
                )
        return carry

    lax.fori_loop(0, LAYERS * HEADS_DEV, build, 0)

    others = (n_sp - 1) * rows
    pltpu.make_async_copy(
        x_dst.at[pl.ds(0, others)], x_dst.at[pl.ds(0, others)], x_r.at[0]
    ).wait()
    for g in range(GROUPS):
        for s in range(2):
            xg[g, tp, s * TILE : (s + 1) * TILE] = (
                x_dst[g * 8 : (g + 1) * 8, s].astype(F32).reshape(TILE, CH).astype(BF16)
            )

    first, second, whole = pl.ds(0, TILE), pl.ds(TILE, TILE), pl.ds(0, TOK)
    gather = (
        (tp, first, right), (tp, second, right), (left, first, right),
        (tp, second, left), (tp, first, left), (right, second, left),
        (tp, whole, partner), (left, first, partner), (left, second, partner),
        (right, first, partner), (right, second, partner),
        (opp, first, partner), (opp, second, partner),
    )

    def ag(g, k):
        owner, span, target = gather[k]
        ref = xg.at[g, owner, span]
        return remote(ref, ref, ag_s.at[g, k], ag_r.at[g, k], {"tp": target})

    sides = (opp, right, left, tp)

    def die(g, k):
        return remote(part.at[g, k], pd2d.at[g, k], d_s.at[g, k], d_r.at[g, k], {"tp": partner})

    scatter = (
        (0, first, right), (0, second, left), (1, second, right),
        (2, first, left), (1, first, right), (2, second, left),
    )

    def ring(g, k):
        side, span, target = scatter[k]
        return remote(ssum.at[g, side, span], rs_y.at[g, k], y_s.at[g, k], y_r.at[g, k], {"tp": target})

    def halo(g, par, s):
        return remote(
            kv.at[par, 1 + s, g], kv.at[par, 3 * (1 - s), g], h_s.at[par, g, s], h_r.at[par, g, s],
            {"sp": (sp + 2 * s - 1 + n_sp) % n_sp},
        )

    lane_head = lax.broadcasted_iota(jnp.int32, (TILE, CH), 1) // HEAD_DIM
    head_mask = [(lane_head == h).astype(F32).astype(BF16) for h in range(HEADS_DEV)]

    def start_own(g):
        for k in (0, 3, 6, 1, 4):
            ag(g, k).start()

    def arrive(g, k, *onward):
        ag(g, k).wait_recv()
        for j in onward:
            ag(g, j).start()

    def accumulate(g, l, blocks, fresh):
        total = None
        squares = None
        for b in blocks:
            wide = xg[g, b].astype(F32)
            sq_b = wide * wide
            sq_b = sq_b[:, :128] + sq_b[:, 128:]
            squares = sq_b if squares is None else squares + sq_b
            term = dot((wide * gains[l, b]).astype(BF16), wqkv[l, b])
            total = term if total is None else total + term
        if fresh:
            acc[g] = total
            sq[g] = squares
        else:
            acc[g] += total
            sq[g] += squares

    def q1(g):
        arrive(g, 0, 2, 7)
        arrive(g, 3, 5, 10)

    def q2(g, l):
        arrive(g, 6)
        accumulate(g, l, (tp, partner), True)
        arrive(g, 1, 8)
        arrive(g, 4, 9)
        accumulate(g, l, (left, right), False)

    def q3(g, l):
        arrive(g, 2, 11)
        arrive(g, 5, 12)
        for k in (7, 8, 9, 10):
            arrive(g, k)
        accumulate(g, l, (left + flip, right + flip), False)

    def q4(g, l, par):
        arrive(g, 11)
        arrive(g, 12)
        accumulate(g, l, (opp, opp + flip), False)
        inverse = lax.rsqrt(jnp.sum(sq[g], axis=1, keepdims=True) / D + EPS)
        for s in range(2):
            piece = slice(s * TILE, (s + 1) * TILE)
            kv[par, 1 + s, g] = (acc[g, piece, CH:] * inverse[piece]).astype(BF16)
            halo(g, par, s).start()
        qs[g] = (acc[g, :, :CH] * (inverse * HEAD_DIM**-0.5)).astype(BF16)
        for k in range(13):
            ag(g, k).wait_send()

    def halo_in(g, par):
        for s in range(2):
            halo(g, par, s).wait_recv()

    def window(par, slot, g, lo):
        up, down = (g + 3) % 4, (g + 1) % 4
        return jnp.concatenate(
            [
                kv[par, slot, up, TILE // 2 :, lo : lo + CH],
                kv[par, slot, g, :, lo : lo + CH],
                kv[par, slot, down, : TILE // 2, lo : lo + CH],
            ],
            axis=0,
        )

    def attend(g, l, par):
        for s in range(2):
            q = qs[g, s * TILE : (s + 1) * TILE, :]
            q_all = jnp.concatenate([q * m for m in head_mask], axis=0)
            table = bias[pl.ds(HEADS_DEV * l, HEADS_DEV)].reshape(HEADS_DEV * TILE, 3 * 128)
            scores = jnp.concatenate(
                [dot_nt(q_all, window(par, s + j, g, 0)) for j in range(3)], axis=1
            ) + table
            highest = jnp.max(scores, axis=1, keepdims=True)
            weights = jnp.exp(scores - highest)
            total = jnp.sum(weights, axis=1, keepdims=True)
            weights = weights.astype(BF16)
            values = jnp.concatenate([window(par, s + j, g, CH) for j in range(3)], axis=0)
            o = dot(weights, values) / total
            out = o[:TILE]
            for h in range(1, HEADS_DEV):
                out = jnp.where(lane_head == h, o[h * TILE : (h + 1) * TILE], out)
            mixed[g, s * TILE : (s + 1) * TILE, :] = out.astype(BF16)

    def p1(g, l):
        for k in range(4):
            part[g, k] = dot(mixed[g], wout[l, sides[k] + flip]).astype(BF16)
            die(g, k).start()

    def pair(g, l, k):
        mine = dot(mixed[g], wout[l, sides[k]])
        die(g, k).wait_recv()
        return mine + pd2d[g, k].astype(F32)

    def p2(g, l):
        ssum[g, 0] = pair(g, l, 0).astype(BF16)
        ring(g, 0).start()
        ring(g, 1).start()
        ssum[g, 1] = pair(g, l, 1).astype(BF16)
        ring(g, 2).start()
        ssum[g, 2] = pair(g, l, 2).astype(BF16)
        ring(g, 3).start()
        own[g] = pair(g, l, 3) + xg[g, tp].astype(F32)

    def p3(g):
        for k, span in ((0, first), (1, second)):
            ring(g, k).wait_recv()
            side = 1 + k
            ssum[g, side, span] = (
                ssum[g, side, span].astype(F32) + rs_y[g, k].astype(F32)
            ).astype(BF16)
            ring(g, 4 + k).start()

    def out_copy(g, r):
        row = 8 * g + r
        return remote(
            o_src.at[row], o_dst.at[sp, row % rows], o_s.at[0], o_r.at[0], {"sp": row // rows}
        )

    def p4(g, l):
        for k in (2, 3, 4, 5):
            ring(g, k).wait_recv()
        top = own[g, first] + rs_y[g, 4].astype(F32) + rs_y[g, 3].astype(F32)
        low = own[g, second] + rs_y[g, 2].astype(F32) + rs_y[g, 5].astype(F32)
        for k in range(4):
            die(g, k).wait_send()
        for k in range(6):
            ring(g, k).wait_send()

        @pl.when(l < LAYERS - 1)
        def _():
            xg[g, tp, first] = top.astype(BF16)
            xg[g, tp, second] = low.astype(BF16)
            start_own(g)

        @pl.when(l == LAYERS - 1)
        def _():
            for s, piece in enumerate((top, low)):
                o_src[pl.ds(8 * g, 8), s] = piece.reshape(8, STRIP_C, CH).astype(BF16)

            def send(r, carry):
                row = 8 * g + r

                @pl.when(row // rows != sp)
                def _():
                    out_copy(g, r).start()

                @pl.when(row // rows == sp)
                def _():
                    o_dst[sp, row % rows] = o_src[row]

                return carry

            lax.fori_loop(0, 8, send, 0)

    start_own(0)
    start_own(1)

    def layer(l, carry):
        par = l % 2
        a, b, c, d = (l % 4, (l + 1) % 4, (l + 2) % 4, (l + 3) % 4)
        for copy in weight_copies(l):
            copy.wait()

        def refill(g):
            @pl.when(l == 0)
            def _():
                start_own(g)

            @pl.when(l > 0)
            def _():
                p4(g, l - 1)

        q1(a)

        @pl.when(l > 0)
        def _():
            p3(d)

        refill(c)
        q1(b)
        q2(a, l)
        refill(d)
        q3(a, l)
        q2(b, l)
        q1(c)
        q4(a, l, par)
        q3(b, l)
        q2(c, l)
        q1(d)
        q4(b, l, par)
        q3(c, l)
        q2(d, l)
        q4(c, l, par)
        halo_in(a, par)
        halo_in(b, par)
        q3(d, l)
        halo_in(c, par)
        attend(b, l, par)
        p1(b, l)
        q4(d, l, par)
        p2(b, l)
        halo_in(d, par)
        attend(c, l, par)
        p1(c, l)
        p3(b)
        p2(c, l)
        attend(d, l, par)
        p1(d, l)
        p4(b, l)
        p3(c)
        p2(d, l)
        attend(a, l, par)
        p1(a, l)
        p4(c, l)
        p3(d)
        p2(a, l)
        for g in range(GROUPS):
            for s in range(2):
                halo(g, par, s).wait_send()
        return carry

    lax.fori_loop(0, LAYERS, layer, 0)
    last = LAYERS - 1
    p3(last % 4)
    p4((last + 3) % 4, last)
    p4(last % 4, last)

    pltpu.make_async_copy(
        x_src.at[pl.ds(0, n_sp - 1)], x_src.at[pl.ds(0, n_sp - 1)], x_s.at[0]
    ).wait()
    gone = ROWS - rows
    pltpu.make_async_copy(o_src.at[pl.ds(0, gone)], o_src.at[pl.ds(0, gone)], o_s.at[0]).wait()
    pltpu.make_async_copy(
        o_dst.at[pl.ds(0, n_sp - 1)], o_dst.at[pl.ds(0, n_sp - 1)], o_r.at[0]
    ).wait()
    for r in range(rows):
        out_ref[r] = o_dst[:, r].astype(F32).reshape(n_sp * WIN_C, CH).T.astype(BF16)


def body(token_grid, norm_gain, w_query, w_key, w_value, w_out, rel_bias):
    n_sp = lax.axis_size("sp")
    rows = token_grid.shape[0]
    wq, wk, wv = (w.reshape(LAYERS, N_TP, CH, CH) for w in (w_query, w_key, w_value))
    vmem = pl.BlockSpec(memory_space=pltpu.VMEM)
    hbm = pl.BlockSpec(memory_space=pl.ANY)
    dma = pltpu.SemaphoreType.DMA
    return pl.pallas_call(
        functools.partial(kernel, n_sp, rows),
        out_shape=jax.ShapeDtypeStruct(token_grid.shape, BF16),
        in_specs=[vmem, vmem, vmem, hbm, hbm, hbm, hbm],
        out_specs=vmem,
        scratch_shapes=[
            pltpu.VMEM((n_sp, rows, 2, STRIP_C, CH), BF16),
            pltpu.VMEM((ROWS, 2, STRIP_C, CH), BF16),
            pltpu.VMEM((ROWS, 2, STRIP_C, CH), BF16),
            pltpu.VMEM((n_sp, rows, 2, STRIP_C, CH), BF16),
            pltpu.VMEM((LAYERS, N_TP, CH, 3 * CH), BF16),
            pltpu.VMEM((LAYERS, N_TP, CH, CH), BF16),
            pltpu.VMEM((LAYERS, N_TP, 1, CH), F32),
            pltpu.VMEM((LAYERS * HEADS_DEV, WIN_R, 128), F32),
            pltpu.VMEM((LAYERS * HEADS_DEV, TILE, 3 * 128), F32),
            pltpu.VMEM((GROUPS, N_TP, TOK, CH), BF16),
            pltpu.VMEM((GROUPS, TOK, 3 * CH), F32),
            pltpu.VMEM((GROUPS, TOK, 128), F32),
            pltpu.VMEM((GROUPS, TOK, CH), BF16),
            pltpu.VMEM((2, 4, GROUPS, TILE, 2 * CH), BF16),
            pltpu.VMEM((GROUPS, TOK, CH), BF16),
            pltpu.VMEM((GROUPS, 4, TOK, CH), BF16),
            pltpu.VMEM((GROUPS, 3, TOK, CH), BF16),
            pltpu.VMEM((GROUPS, TOK, CH), F32),
            pltpu.VMEM((GROUPS, 4, TOK, CH), BF16),
            pltpu.VMEM((GROUPS, 6, TILE, CH), BF16),
            dma((LAYERS, 3 + N_TP)), dma((1,)), dma((1,)), dma((1,)), dma((1,)),
            dma((GROUPS, 13)), dma((GROUPS, 13)), dma((GROUPS, 4)), dma((GROUPS, 4)),
            dma((GROUPS, 6)), dma((GROUPS, 6)), dma((2, GROUPS, 2)), dma((2, GROUPS, 2)),
        ],
        compiler_params=pltpu.CompilerParams(
            collective_id=0, has_side_effects=True, vmem_limit_bytes=60 * 1024 * 1024
        ),
    )(token_grid, norm_gain, rel_bias, wq, wk, wv, w_out)


def solution(mesh):
    in_specs = (
        P("sp", "tp", None),
        P(),
        P(None, None, "tp"),
        P(None, None, "tp"),
        P(None, None, "tp"),
        P(None, "tp", None),
        P(None, "tp", None, None),
    )
    out_specs = P("sp", "tp", None)
    return jax.shard_map(body, mesh=mesh, in_specs=in_specs, out_specs=out_specs, check_vma=False)
```

time: 542 us -> 141 us (0.26)
  waiting for transfers between devices: 255 us -> 0 us
  Pallas kernels: 0 us -> 136 us
  other arithmetic: 129 us -> 0 us
  blocking collectives: 58.3 us -> 0 us
  starting transfers between devices: 53.9 us -> 0 us
  local copies, waits for them, and re-layouts: 21.6 us -> 1.67 us
  matrix products: 15.6 us -> 0 us
    ppermute x21 -> x0, waiting for transfers between devices: 156 us -> none  [from_behind(): return lax.ppermute(block, axis, route)]
    pallas_call x0 -> x1, Pallas kernels: none -> 136 us  [body(): pl.pallas_call(functools.partial(kernel, n_sp, rows), out_shape=jax.Shape...]
    all_to_all x4 -> x0, waiting for transfers between devices: 99.5 us -> none  [the longest x3 73.4 us: copy_for_each(): lax.all_to_all(jnp.broadcast_to(x[None], (size, *x.shape)), axis, 0, 0, t...]
    unnamed x54 -> x0, other arithmetic: 62.8 us -> none
    all_to_all x2 -> x0, blocking collectives: 58.3 us -> none  [sent_and_summed(): lax.all_to_all(pieces, axis, split_axis=0, concat_axis=0, tiled=True)]
    dot_general x12 -> x0, other arithmetic: 52.2 us -> none  [body(): jnp.einsum('shc,shdc->hdc', weights[offset], shifted, preferred_element_t...]
    ppermute x21 -> x0, starting transfers between devices: 34.2 us -> none  [from_behind(): return lax.ppermute(block, axis, route)]
    all_to_all x4 -> x0, starting transfers between devices: 19.7 us -> none  [the longest x3 15.7 us: copy_for_each(): lax.all_to_all(jnp.broadcast_to(x[None], (size, *x.shape)), axis, 0, 0, t...]
  transfers between devices with their start and end apart: 25 -> 0, of which waited for: 16 -> 0; matrix products, arithmetic and copies ran while one was open for 2% -> 0% of each run, Pallas kernels for 0% -> 0%
where the time goes in v2:
time: 141 us; the launch traced here: 138 us
  Pallas kernels  136 us (96%)
  local copies, waits for them, and re-layouts  1.67 us (1%)
    pallas_call x1, Pallas kernels, body(): pl.pallas_call(functools.partial(kernel, n_sp, rows), out_shape=jax.Shape...  136 us

profile of v2, /device:TPU:1, one launch (start us, length us, event | category | flops | bytes accessed | tf_op | source)
XLA Modules:
  0.0 138.2 jit_solution(10065420034646602772)
XLA Ops:
  0.0 136.5 %shard_map.73 = bf16[1,256,512]{2,1,0:T(8,128)(2,1)} custom-call(bf16[1,256,512]{2,1,0:T(8,128)(2,1)} %x_ref.1, bf16[3,2048]{1,0:T(4,128)(2,1)} %gain_ref.1, f32[3,4,8,16]{3,2,1,0:T(8,128)} %bias_ref.1, bf16[3,8,256,256]{3,2,1,0:T(8,128)(2,1)} %bitcast.3, bf16[3,8,256,256]{3,2,1,0:T(8,128)(2,1)} %bitcast.4, bf16[3,8,256,256]{3,2,1,0:T(8,128)(2,1)} %bitcast.5, ...), custom_call_target="tpu_custom_call" | custom-call | tf_op jit(solution)/shard_map/pallas_call | solution.py:437
  136.5 1.7 %copy.9 = bf16[1,256,512]{2,1,0:T(8,128)(2,1)} copy(bf16[1,256,512]{2,1,0:T(8,128)(2,1)} %shard_map.73) | data formatting | bytes 524288

commit v3 on v0

v3 whole, which is shorter than its diff:
```python
import functools

import jax
import jax.numpy as jnp
from jax import lax
from jax.experimental import pallas as pl
from jax.experimental.pallas import tpu as pltpu
from jax.sharding import PartitionSpec as P

D = 2048
HEAD_DIM = 64
CH = 256
PAIR = 2 * CH
N_TP = 8
CHIPS = 4
WIN_R = 8
WIN_C = 16
LAYERS = 3
HEADS = 8
ROWS = 32
GROUPS = 4
STRIP_C = 8
TILE = 64
EPS = 1e-06
NEG = -1e30
MESH = pl.DeviceIdType.MESH
F32 = jnp.float32
BF16 = jnp.bfloat16

OWN, RELAY, MINE, SIDES, FAR, ATTEND, PROJECT, ADD, FINISH = range(9)
ORDER = (
    (OWN, 0, 1), (OWN, 0, 3), (OWN, 0, 0), (MINE, 0, 1), (MINE, 0, 3),
    (OWN, 0, 2), (MINE, 0, 0), (MINE, 0, 2), (RELAY, 0, 1), (RELAY, 0, 3),
    (SIDES, 0, 1), (SIDES, 0, 3), (RELAY, 0, 0), (SIDES, 0, 0), (RELAY, 0, 2),
    (FAR, 0, 1), (FAR, 0, 3), (FAR, 0, 0), (SIDES, 0, 2), (FAR, 0, 2),
    (ATTEND, 0, 0), (PROJECT, 0, 0), (ATTEND, 0, 1), (PROJECT, 0, 1), (ATTEND, 0, 3),
    (PROJECT, 0, 3), (ADD, 0, 0), (ATTEND, 0, 2), (PROJECT, 0, 2), (ADD, 0, 1),
    (ADD, 0, 3), (FINISH, 0, 0), (MINE, 1, 0), (ADD, 0, 2), (FINISH, 0, 1),
    (FINISH, 0, 3), (RELAY, 1, 0), (MINE, 1, 1), (MINE, 1, 3), (SIDES, 1, 0),
    (RELAY, 1, 1), (FINISH, 0, 2), (MINE, 1, 2), (RELAY, 1, 3), (SIDES, 1, 1),
    (FAR, 1, 0), (FAR, 1, 1), (RELAY, 1, 2), (SIDES, 1, 3), (SIDES, 1, 2),
    (FAR, 1, 3), (FAR, 1, 2), (ATTEND, 1, 0), (PROJECT, 1, 0), (ATTEND, 1, 2),
    (PROJECT, 1, 2), (ATTEND, 1, 1), (PROJECT, 1, 1), (ADD, 1, 0), (ATTEND, 1, 3),
    (PROJECT, 1, 3), (ADD, 1, 2), (ADD, 1, 1), (FINISH, 1, 0), (MINE, 2, 0),
    (ADD, 1, 3), (FINISH, 1, 2), (MINE, 2, 2), (FINISH, 1, 1), (RELAY, 2, 0),
    (MINE, 2, 1), (SIDES, 2, 0), (RELAY, 2, 2), (FINISH, 1, 3), (MINE, 2, 3),
    (SIDES, 2, 2), (RELAY, 2, 1), (FAR, 2, 0), (FAR, 2, 2), (RELAY, 2, 3),
    (SIDES, 2, 3), (SIDES, 2, 1), (FAR, 2, 1), (FAR, 2, 3), (ATTEND, 2, 1),
    (PROJECT, 2, 1), (ATTEND, 2, 3), (PROJECT, 2, 3), (ATTEND, 2, 2), (PROJECT, 2, 2),
    (ATTEND, 2, 0), (PROJECT, 2, 0), (ADD, 2, 3), (ADD, 2, 1), (ADD, 2, 2),
    (ADD, 2, 0), (FINISH, 2, 3), (FINISH, 2, 1), (FINISH, 2, 2), (FINISH, 2, 0),
)


def dot(a, b):
    return lax.dot_general(a, b, (((1,), (0,)), ((), ())), preferred_element_type=F32)


def dot_nt(a, b):
    return lax.dot_general(a, b, (((1,), (1,)), ((), ())), preferred_element_type=F32)


def kernel(
    n_sp, rows, x_ref, gain_ref, bias_ref, wq_ref, wk_ref, wv_ref, wo_ref, out_ref,
    x_src, x_dst, o_src, o_dst, wqkv, wout, gains, heads, pad, bias,
    xg, acc, sq, qs, kv, mixed, ssum, own, rs_y,
    w_sem, wr_s, wr_r, b_s, b_r, x_s, x_r, o_s, o_r, ag_s, ag_r, y_s, y_r, h_s, h_r,
):
    tp = lax.axis_index("tp")
    sp = lax.axis_index("sp")
    y, core = tp // 2, tp % 2
    right, left, opp = (y + 1) % 4, (y + 3) % 4, (y + 2) % 4
    partner = y * 2 + 1 - core

    barrier = pltpu.get_barrier_semaphore()
    for target in (right * 2 + core, left * 2 + core, partner):
        pl.semaphore_signal(barrier, inc=1, device_id={"tp": target}, device_id_type=MESH)

    def greet(i, carry):
        there = (sp + i) % n_sp
        pl.semaphore_signal(barrier, inc=1, device_id={"sp": there}, device_id_type=MESH)
        pl.semaphore_signal(
            barrier, inc=1, device_id={"sp": there, "tp": partner}, device_id_type=MESH
        )
        return carry

    lax.fori_loop(1, n_sp, greet, 0)

    def remote(src, dst, s_sem, r_sem, target):
        return pltpu.make_async_remote_copy(
            src_ref=src, dst_ref=dst, send_sem=s_sem, recv_sem=r_sem,
            device_id=target, device_id_type=MESH,
        )

    def weight_pairs(l):
        pairs = []
        for i, ref in enumerate((wq_ref, wk_ref, wv_ref)):
            lanes = pl.ds(pl.multiple_of(i * PAIR + core * CH, CH), CH)
            pairs.append((ref.at[l], wqkv.at[l, :, :, lanes]))
        for b in range(CHIPS):
            pairs.append(
                (wo_ref.at[l, :, pl.ds(b * PAIR, PAIR)], wout.at[l, b, pl.ds(core * CH, CH)])
            )
        return pairs

    def weights_here(l, i):
        src, dst = weight_pairs(l)[i]
        return pltpu.make_async_copy(src, dst, w_sem.at[l, i])

    def weights_across(l, i):
        src, dst = weight_pairs(l)[i]
        return remote(src, dst, wr_s.at[l, i], wr_r.at[l, i], {"tp": partner})

    parts = 3 + CHIPS
    for l in range(LAYERS):
        for i in range(parts):
            weights_here(l, i).start()

    for r in range(rows):
        turned = x_ref[r].astype(F32).T.reshape(n_sp, 2, STRIP_C, CH).astype(BF16)
        for c in range(2):
            x_src[:, c, r] = turned[:, c]

    here = pl.ds(sp * rows, rows)

    def scatter_in(i, carry):
        there = (sp + i) % n_sp

        @pl.when(i > 0)
        def _():
            remote(
                x_src.at[there, core], x_dst.at[core, here], x_s.at[0], x_r.at[core], {"sp": there}
            ).start()

        remote(
            x_src.at[there, 1 - core], x_dst.at[core, here], x_s.at[1], x_r.at[core],
            {"sp": there, "tp": partner},
        ).start()
        return carry

    pl.semaphore_wait(barrier, 2 * n_sp + 1)
    lax.fori_loop(0, n_sp, scatter_in, 0)
    bias_copy = remote(bias_ref, heads.at[core], b_s.at[0], b_r.at[0], {"tp": partner})
    bias_copy.start()
    for i in range(parts):
        weights_across(0, i).start()
    x_dst[core, here] = x_src[sp, core]
    heads[core] = bias_ref[...]

    for l in range(LAYERS):
        for b in range(N_TP):
            gains[l, b] = gain_ref[l : l + 1, b * CH : (b + 1) * CH].astype(F32)
    pad[...] = jnp.zeros_like(pad)
    bias_copy.wait()
    for l in range(LAYERS):
        for h in range(HEADS):
            pad[l, h, :, :WIN_C] = heads[h // 4, l, h % 4]
    lane = lax.broadcasted_iota(jnp.int32, (8, 128), 1)
    lane_c = lane % STRIP_C
    row_c = lax.broadcasted_iota(jnp.int32, (8, 128), 0)
    nothing = jnp.full((8, 128), NEG, F32)

    def build(l, carry):
        for h in range(HEADS):
            table = pad[l, h]
            lanes = []
            for j in range(2):
                piece = table if j == 0 else pltpu.roll(table, 128 - STRIP_C, 1)
                piece = jnp.where(lane < STRIP_C, piece, 0.0)
                piece = pltpu.roll(piece, 0, 1, stride=STRIP_C, stride_axis=0)
                piece = jnp.broadcast_to(jnp.sum(piece, axis=0, keepdims=True), (8, 128))
                lanes.append(jnp.where(lane < WIN_R * STRIP_C, piece, NEG))
            straight = [pltpu.roll(g, 0, 1, stride=1, stride_axis=0) for g in lanes] + [nothing]
            carried = [nothing] + [
                pltpu.roll(g, 128 - STRIP_C, 1, stride=1, stride_axis=0) for g in lanes
            ]
            for j in range(3):
                t = jnp.where(lane_c >= row_c, straight[j], carried[j])
                for r in range(8):
                    bias[l, h, r * 8 : (r + 1) * 8, j * 128 : (j + 1) * 128] = (
                        t if r == 0 else pltpu.roll(t, r * STRIP_C, 1)
                    )
        return carry

    lax.fori_loop(0, LAYERS, build, 0)

    most = x_dst.at[core, pl.ds(0, ROWS - rows)]
    pltpu.make_async_copy(most, most, x_r.at[core]).wait()
    rest = x_dst.at[1 - core]
    pltpu.make_async_copy(rest, rest, x_r.at[1 - core]).wait()
    for g in range(GROUPS):
        for h in range(2):
            xg[g, y, h] = (
                x_dst[h, g * 8 : (g + 1) * 8].astype(F32).reshape(TILE, CH).astype(BF16)
            )

    to_right, to_left = right * 2 + core, left * 2 + core
    gather = (
        (y, 0, to_right), (y, 1, to_right), (left, 0, to_right),
        (y, 1, to_left), (y, 0, to_left), (right, 1, to_left),
    )

    def ag(g, k):
        owner, half, target = gather[k]
        ref = xg.at[g, owner, half]
        return remote(ref, ref, ag_s.at[g, k], ag_r.at[g, k], {"tp": target})

    sides = (opp, right, left, y)
    scatter = (
        (0, 0, to_right), (0, 1, to_left), (1, 1, to_right),
        (2, 0, to_left), (1, 0, to_right), (2, 1, to_left),
    )

    def ring(g, k):
        side, half, target = scatter[k]
        return remote(
            ssum.at[g, side, half], rs_y.at[g, k], y_s.at[g, k], y_r.at[g, k], {"tp": target}
        )

    def halo(par, g, k):
        slot = 2 * core if k else 2 * (1 - core)
        target = {"tp": partner}
        if k == 0:
            target["sp"] = (sp + 2 * core - 1 + n_sp) % n_sp
        return remote(kv.at[par, 1, g], kv.at[par, slot, g], h_s.at[par, g, k], h_r.at[par, g, k], target)

    lane_head = lax.broadcasted_iota(jnp.int32, (TILE, CH), 1) // HEAD_DIM
    head_mask = [(lane_head == h).astype(F32).astype(BF16) for h in range(4)]

    def start_own(g):
        for k in (0, 3, 1, 4):
            ag(g, k).start()

    def step_own(l, g):
        start_own(g)

    def step_relay(l, g):
        for k, onward in ((0, 2), (3, 5)):
            ag(g, k).wait_recv()
            ag(g, onward).start()

    def accumulate(l, g, blocks, fresh):
        total = None
        squares = None
        for chip, half in blocks:
            wide = xg[g, chip, half].astype(F32)
            sq_b = wide * wide
            sq_b = sq_b[:, :128] + sq_b[:, 128:]
            squares = sq_b if squares is None else squares + sq_b
            b = chip * 2 + half
            term = dot((wide * gains[l, b]).astype(BF16), wqkv[l, b])
            total = term if total is None else total + term
        if fresh:
            acc[g] = total
            sq[g] = squares
        else:
            acc[g] += total
            sq[g] += squares

    ready = set()

    def weights_in(l, which, parts_of):
        if (l, which) in ready:
            return
        ready.add((l, which))
        for i in parts_of:
            weights_here(l, i).wait()
            weights_across(l, i).wait_recv()

    def step_mine(l, g):
        weights_in(l, 0, range(3))
        accumulate(l, g, ((y, 0), (y, 1)), True)

    def step_sides(l, g):
        ag(g, 1).wait_recv()
        ag(g, 4).wait_recv()
        accumulate(l, g, ((left, 0), (right, 1), (left, 1), (right, 0)), False)

    def step_far(l, g):
        par = l % 2
        ag(g, 2).wait_recv()
        ag(g, 5).wait_recv()
        accumulate(l, g, ((opp, 0), (opp, 1)), False)
        inverse = lax.rsqrt(jnp.sum(sq[g], axis=1, keepdims=True) / D + EPS)
        if l >= 2:
            for k in range(2):
                halo(par, g, k).wait_send()
        kv[par, 1, g] = (acc[g, :, PAIR:] * inverse).astype(BF16)
        for k in range(2):
            halo(par, g, k).start()
        qs[g] = (acc[g, :, :PAIR] * (inverse * HEAD_DIM**-0.5)).astype(BF16)
        for k in range(6):
            ag(g, k).wait_send()

    def window(par, slot, g, lo):
        up, down = (g + 3) % 4, (g + 1) % 4
        return jnp.concatenate(
            [
                kv[par, slot, up, TILE // 2 :, lo : lo + CH],
                kv[par, slot, g, :, lo : lo + CH],
                kv[par, slot, down, : TILE // 2, lo : lo + CH],
            ],
            axis=0,
        )

    def step_attend(l, g):
        par = l % 2
        for near in ((g + 3) % 4, g, (g + 1) % 4):
            if (l, near, "halo") not in ready:
                ready.add((l, near, "halo"))
                for k in range(2):
                    halo(par, near, k).wait_recv()
        for c in range(2):
            lo = c * CH
            q = qs[g, :, lo : lo + CH]
            q_all = jnp.concatenate([q * m for m in head_mask], axis=0)
            table = bias[l, 4 * c : 4 * c + 4].reshape(4 * TILE, 3 * 128)
            scores = jnp.concatenate(
                [dot_nt(q_all, window(par, j, g, lo)) for j in range(3)], axis=1
            ) + table
            highest = jnp.max(scores, axis=1, keepdims=True)
            weights = jnp.exp(scores - highest)
            total = jnp.sum(weights, axis=1, keepdims=True)
            weights = weights.astype(BF16)
            values = jnp.concatenate([window(par, j, g, PAIR + lo) for j in range(3)], axis=0)
            o = dot(weights, values) / total
            out = o[:TILE]
            for h in range(1, 4):
                out = jnp.where(lane_head == h, o[h * TILE : (h + 1) * TILE], out)
            mixed[g, :, lo : lo + CH] = out.astype(BF16)
        if l < LAYERS - 1 and (l, "across") not in ready:
            ready.add((l, "across"))
            for i in range(parts):
                weights_across(l + 1, i).start()

    def step_project(l, g):
        weights_in(l, 1, range(3, parts))
        m = mixed[g]
        for k in range(3):
            piece = dot(m, wout[l, sides[k]]).astype(BF16)
            for half in range(2):
                ssum[g, k, half] = piece[:, half * CH : (half + 1) * CH]
        for k in range(4):
            ring(g, k).start()
        piece = dot(m, wout[l, y])
        for half in range(2):
            own[g, half] = piece[:, half * CH : (half + 1) * CH] + xg[g, y, half].astype(F32)

    def step_add(l, g):
        for k in range(2):
            ring(g, k).wait_recv()
            side = 1 + k
            ssum[g, side, k] = (ssum[g, side, k].astype(F32) + rs_y[g, k].astype(F32)).astype(BF16)
            ring(g, 4 + k).start()

    def step_finish(l, g):
        for k in (2, 3, 4, 5):
            ring(g, k).wait_recv()
        new = (
            own[g, 0] + rs_y[g, 4].astype(F32) + rs_y[g, 3].astype(F32),
            own[g, 1] + rs_y[g, 2].astype(F32) + rs_y[g, 5].astype(F32),
        )
        if l < LAYERS - 1:
            for half in range(2):
                xg[g, y, half] = new[half].astype(BF16)
            start_own(g)
        else:
            for half in range(2):
                o_src[half, 8 * g : 8 * g + 8] = new[half].reshape(8, STRIP_C, CH).astype(BF16)

            def send(r, carry):
                row = 8 * g + r
                there, spot = row // rows, row % rows

                @pl.when(there != sp)
                def _():
                    remote(
                        o_src.at[core, row], o_dst.at[core, sp, spot], o_s.at[0], o_r.at[core],
                        {"sp": there},
                    ).start()

                @pl.when(there == sp)
                def _():
                    o_dst[core, sp, spot] = o_src[core, row]

                remote(
                    o_src.at[1 - core, row], o_dst.at[core, sp, spot], o_s.at[1], o_r.at[core],
                    {"sp": there, "tp": partner},
                ).start()
                return carry

            lax.fori_loop(0, 8, send, 0)
        for k in range(6):
            ring(g, k).wait_send()

    steps = (
        step_own, step_relay, step_mine, step_sides, step_far,
        step_attend, step_project, step_add, step_finish,
    )
    for step, l, g in ORDER:
        steps[step](l, g)

    for l in range(LAYERS):
        for i in range(parts):
            weights_across(l, i).wait_send()
    for l in range(1, LAYERS):
        for g in range(GROUPS):
            for k in range(2):
                halo(l % 2, g, k).wait_send()
    gone = x_src.at[pl.ds(0, n_sp - 1), core]
    pltpu.make_async_copy(gone, gone, x_s.at[0]).wait()
    gone = x_src.at[:, core]
    pltpu.make_async_copy(gone, gone, x_s.at[1]).wait()
    gone = o_src.at[core, pl.ds(0, ROWS - rows)]
    pltpu.make_async_copy(gone, gone, o_s.at[0]).wait()
    gone = o_src.at[1 - core]
    pltpu.make_async_copy(gone, gone, o_s.at[1]).wait()
    most = o_dst.at[core, pl.ds(0, n_sp - 1)]
    pltpu.make_async_copy(most, most, o_r.at[core]).wait()
    rest = o_dst.at[1 - core]
    pltpu.make_async_copy(rest, rest, o_r.at[1 - core]).wait()
    for r in range(rows):
        both = jnp.stack([o_dst[c, :, r].astype(F32) for c in range(2)], axis=1)
        out_ref[r] = both.reshape(n_sp * WIN_C, CH).T.astype(BF16)


def body(token_grid, norm_gain, w_query, w_key, w_value, w_out, rel_bias):
    n_sp = lax.axis_size("sp")
    rows = token_grid.shape[0]
    wq, wk, wv = (w.reshape(LAYERS, N_TP, CH, CH) for w in (w_query, w_key, w_value))
    vmem = pl.BlockSpec(memory_space=pltpu.VMEM)
    hbm = pl.BlockSpec(memory_space=pl.ANY)
    dma = pltpu.SemaphoreType.DMA
    parts = 3 + CHIPS
    return pl.pallas_call(
        functools.partial(kernel, n_sp, rows),
        out_shape=jax.ShapeDtypeStruct(token_grid.shape, BF16),
        in_specs=[vmem, vmem, vmem, hbm, hbm, hbm, hbm],
        out_specs=vmem,
        scratch_shapes=[
            pltpu.VMEM((n_sp, 2, rows, STRIP_C, CH), BF16),
            pltpu.VMEM((2, ROWS, STRIP_C, CH), BF16),
            pltpu.VMEM((2, ROWS, STRIP_C, CH), BF16),
            pltpu.VMEM((2, n_sp, rows, STRIP_C, CH), BF16),
            pltpu.VMEM((LAYERS, N_TP, CH, 3 * PAIR), BF16),
            pltpu.VMEM((LAYERS, CHIPS, PAIR, PAIR), BF16),
            pltpu.VMEM((LAYERS, N_TP, 1, CH), F32),
            pltpu.VMEM((2, LAYERS, 4, WIN_R, WIN_C), F32),
            pltpu.VMEM((LAYERS, HEADS, WIN_R, 128), F32),
            pltpu.VMEM((LAYERS, HEADS, TILE, 3 * 128), F32),
            pltpu.VMEM((GROUPS, CHIPS, 2, TILE, CH), BF16),
            pltpu.VMEM((GROUPS, TILE, 3 * PAIR), F32),
            pltpu.VMEM((GROUPS, TILE, 128), F32),
            pltpu.VMEM((GROUPS, TILE, PAIR), BF16),
            pltpu.VMEM((2, 3, GROUPS, TILE, 2 * PAIR), BF16),
            pltpu.VMEM((GROUPS, TILE, PAIR), BF16),
            pltpu.VMEM((GROUPS, 3, 2, TILE, CH), BF16),
            pltpu.VMEM((GROUPS, 2, TILE, CH), F32),
            pltpu.VMEM((GROUPS, 6, TILE, CH), BF16),
            dma((LAYERS, parts)), dma((LAYERS, parts)), dma((LAYERS, parts)),
            dma((1,)), dma((1,)), dma((2,)), dma((2,)), dma((2,)), dma((2,)),
            dma((GROUPS, 6)), dma((GROUPS, 6)), dma((GROUPS, 6)), dma((GROUPS, 6)),
            dma((2, GROUPS, 2)), dma((2, GROUPS, 2)),
        ],
        compiler_params=pltpu.CompilerParams(
            collective_id=0, has_side_effects=True, vmem_limit_bytes=60 * 1024 * 1024
        ),
    )(token_grid, norm_gain, rel_bias, wq, wk, wv, w_out)


def solution(mesh):
    in_specs = (
        P("sp", "tp", None),
        P(),
        P(None, None, "tp"),
        P(None, None, "tp"),
        P(None, None, "tp"),
        P(None, "tp", None),
        P(None, "tp", None, None),
    )
    out_specs = P("sp", "tp", None)
    return jax.shard_map(body, mesh=mesh, in_specs=in_specs, out_specs=out_specs, check_vma=False)
```

time: 542 us -> 113 us (0.21); the launches traced: 535 us -> 113 us
  waiting for transfers between devices: 255 us -> 0 us
  other arithmetic: 129 us -> 0 us
  Pallas kernels: 0 us -> 111 us
  blocking collectives: 58.3 us -> 0 us
  starting transfers between devices: 53.9 us -> 0 us
  local copies, waits for them, and re-layouts: 21.6 us -> 1.67 us
  matrix products: 15.6 us -> 0 us
    ppermute x21 -> x0, waiting for transfers between devices: 156 us -> none  [from_behind(): return lax.ppermute(block, axis, route)]
    pallas_call x0 -> x1, Pallas kernels: none -> 111 us  [body(): pl.pallas_call(functools.partial(kernel, n_sp, rows), out_shape=jax.Shape...]
    all_to_all x4 -> x0, waiting for transfers between devices: 99.5 us -> none  [the longest x3 73.4 us: copy_for_each(): lax.all_to_all(jnp.broadcast_to(x[None], (size, *x.shape)), axis, 0, 0, t...]
    unnamed x54 -> x0, other arithmetic: 62.8 us -> none
    all_to_all x2 -> x0, blocking collectives: 58.3 us -> none  [sent_and_summed(): lax.all_to_all(pieces, axis, split_axis=0, concat_axis=0, tiled=True)]
    dot_general x12 -> x0, other arithmetic: 52.2 us -> none  [body(): jnp.einsum('shc,shdc->hdc', weights[offset], shifted, preferred_element_t...]
    ppermute x21 -> x0, starting transfers between devices: 34.2 us -> none  [from_behind(): return lax.ppermute(block, axis, route)]
    all_to_all x4 -> x0, starting transfers between devices: 19.7 us -> none  [the longest x3 15.7 us: copy_for_each(): lax.all_to_all(jnp.broadcast_to(x[None], (size, *x.shape)), axis, 0, 0, t...]
  transfers between devices with their start and end apart: 25 -> 0, of which waited for: 16 -> 0; matrix products, arithmetic and copies ran while one was open for 2% -> 0% of each run, Pallas kernels for 0% -> 0%
where the time goes in v3:
time: 113 us
  Pallas kernels  111 us (98%)
  local copies, waits for them, and re-layouts  1.67 us (1%)
    pallas_call x1, Pallas kernels, body(): pl.pallas_call(functools.partial(kernel, n_sp, rows), out_shape=jax.Shape...  111 us

profile of v3, /device:TPU:1, one launch (start us, length us, event | category | flops | bytes accessed | tf_op | source)
XLA Modules:
  0.0 112.8 jit_solution(9826621431903632112)
XLA Ops:
  0.0 111.2 %shard_map.73 = bf16[1,256,512]{2,1,0:T(8,128)(2,1)} custom-call(bf16[1,256,512]{2,1,0:T(8,128)(2,1)} %x_ref.1, bf16[3,2048]{1,0:T(4,128)(2,1)} %gain_ref.1, f32[3,4,8,16]{3,2,1,0:T(8,128)} %bias_ref.1, bf16[3,8,256,256]{3,2,1,0:T(8,128)(2,1)} %bitcast.3, bf16[3,8,256,256]{3,2,1,0:T(8,128)(2,1)} %bitcast.4, bf16[3,8,256,256]{3,2,1,0:T(8,128)(2,1)} %bitcast.5, ...), custom_call_target="tpu_custom_call" | custom-call | tf_op jit(solution)/shard_map/pallas_call | solution.py:435
  111.2 1.7 %copy.9 = bf16[1,256,512]{2,1,0:T(8,128)(2,1)} copy(bf16[1,256,512]{2,1,0:T(8,128)(2,1)} %shard_map.73) | data formatting | bytes 524288

commit v4 on v3

--- a/solution.py
+++ b/solution.py
@@ -27,28 +27,31 @@
 F32 = jnp.float32
 BF16 = jnp.bfloat16
 
-OWN, RELAY, MINE, SIDES, FAR, ATTEND, PROJECT, ADD, FINISH = range(9)
+OWN, RELAY, MINE, SIDES, FAR, ATTEND, FIRST, REST, ADD, FINISH = range(10)
 ORDER = (
-    (OWN, 0, 1), (OWN, 0, 3), (OWN, 0, 0), (MINE, 0, 1), (MINE, 0, 3),
-    (OWN, 0, 2), (MINE, 0, 0), (MINE, 0, 2), (RELAY, 0, 1), (RELAY, 0, 3),
-    (SIDES, 0, 1), (SIDES, 0, 3), (RELAY, 0, 0), (SIDES, 0, 0), (RELAY, 0, 2),
-    (FAR, 0, 1), (FAR, 0, 3), (FAR, 0, 0), (SIDES, 0, 2), (FAR, 0, 2),
-    (ATTEND, 0, 0), (PROJECT, 0, 0), (ATTEND, 0, 1), (PROJECT, 0, 1), (ATTEND, 0, 3),
-    (PROJECT, 0, 3), (ADD, 0, 0), (ATTEND, 0, 2), (PROJECT, 0, 2), (ADD, 0, 1),
-    (ADD, 0, 3), (FINISH, 0, 0), (MINE, 1, 0), (ADD, 0, 2), (FINISH, 0, 1),
-    (FINISH, 0, 3), (RELAY, 1, 0), (MINE, 1, 1), (MINE, 1, 3), (SIDES, 1, 0),
-    (RELAY, 1, 1), (FINISH, 0, 2), (MINE, 1, 2), (RELAY, 1, 3), (SIDES, 1, 1),
-    (FAR, 1, 0), (FAR, 1, 1), (RELAY, 1, 2), (SIDES, 1, 3), (SIDES, 1, 2),
-    (FAR, 1, 3), (FAR, 1, 2), (ATTEND, 1, 0), (PROJECT, 1, 0), (ATTEND, 1, 2),
-    (PROJECT, 1, 2), (ATTEND, 1, 1), (PROJECT, 1, 1), (ADD, 1, 0), (ATTEND, 1, 3),
-    (PROJECT, 1, 3), (ADD, 1, 2), (ADD, 1, 1), (FINISH, 1, 0), (MINE, 2, 0),
-    (ADD, 1, 3), (FINISH, 1, 2), (MINE, 2, 2), (FINISH, 1, 1), (RELAY, 2, 0),
-    (MINE, 2, 1), (SIDES, 2, 0), (RELAY, 2, 2), (FINISH, 1, 3), (MINE, 2, 3),
-    (SIDES, 2, 2), (RELAY, 2, 1), (FAR, 2, 0), (FAR, 2, 2), (RELAY, 2, 3),
-    (SIDES, 2, 3), (SIDES, 2, 1), (FAR, 2, 1), (FAR, 2, 3), (ATTEND, 2, 1),
-    (PROJECT, 2, 1), (ATTEND, 2, 3), (PROJECT, 2, 3), (ATTEND, 2, 2), (PROJECT, 2, 2),
-    (ATTEND, 2, 0), (PROJECT, 2, 0), (ADD, 2, 3), (ADD, 2, 1), (ADD, 2, 2),
-    (ADD, 2, 0), (FINISH, 2, 3), (FINISH, 2, 1), (FINISH, 2, 2), (FINISH, 2, 0),
+    (OWN, 0, 2), (OWN, 0, 3), (OWN, 0, 0), (OWN, 0, 1), (MINE, 0, 2),
+    (MINE, 0, 3), (MINE, 0, 0), (RELAY, 0, 2), (SIDES, 0, 2), (RELAY, 0, 3),
+    (SIDES, 0, 3), (RELAY, 0, 0), (SIDES, 0, 0), (RELAY, 0, 1), (MINE, 0, 1),
+    (SIDES, 0, 1), (FAR, 0, 2), (FAR, 0, 3), (FAR, 0, 0), (FAR, 0, 1),
+    (ATTEND, 0, 2), (FIRST, 0, 2), (REST, 0, 2), (ATTEND, 0, 3), (FIRST, 0, 3),
+    (REST, 0, 3), (ATTEND, 0, 0), (FIRST, 0, 0), (ADD, 0, 2), (REST, 0, 0),
+    (ATTEND, 0, 1), (FIRST, 0, 1), (ADD, 0, 3), (REST, 0, 1), (ADD, 0, 0),
+    (FINISH, 0, 2), (MINE, 1, 2), (ADD, 0, 1), (FINISH, 0, 3), (MINE, 1, 3),
+    (RELAY, 1, 2), (FINISH, 0, 0), (MINE, 1, 0), (SIDES, 1, 2), (RELAY, 1, 3),
+    (FINISH, 0, 1), (SIDES, 1, 3), (FAR, 1, 2), (RELAY, 1, 0), (SIDES, 1, 0),
+    (FAR, 1, 3), (RELAY, 1, 1), (FAR, 1, 0), (MINE, 1, 1), (SIDES, 1, 1),
+    (FAR, 1, 1), (ATTEND, 1, 2), (FIRST, 1, 2), (REST, 1, 2), (ATTEND, 1, 3),
+    (FIRST, 1, 3), (REST, 1, 3), (ADD, 1, 2), (ATTEND, 1, 0), (FIRST, 1, 0),
+    (REST, 1, 0), (ADD, 1, 3), (ATTEND, 1, 1), (FIRST, 1, 1), (FINISH, 1, 2),
+    (MINE, 2, 2), (ADD, 1, 0), (REST, 1, 1), (FINISH, 1, 3), (ADD, 1, 1),
+    (MINE, 2, 3), (RELAY, 2, 2), (FINISH, 1, 0), (MINE, 2, 0), (SIDES, 2, 2),
+    (RELAY, 2, 3), (FINISH, 1, 1), (MINE, 2, 1), (FAR, 2, 2), (RELAY, 2, 0),
+    (SIDES, 2, 3), (SIDES, 2, 0), (RELAY, 2, 1), (FAR, 2, 3), (SIDES, 2, 1),
+    (FAR, 2, 0), (FAR, 2, 1), (ATTEND, 2, 2), (FIRST, 2, 2), (REST, 2, 2),
+    (ATTEND, 2, 3), (FIRST, 2, 3), (REST, 2, 3), (ATTEND, 2, 0), (FIRST, 2, 0),
+    (REST, 2, 0), (ATTEND, 2, 1), (FIRST, 2, 1), (REST, 2, 1), (ADD, 2, 2),
+    (ADD, 2, 3), (ADD, 2, 0), (ADD, 2, 1), (FINISH, 2, 2), (FINISH, 2, 3),
+    (FINISH, 2, 0), (FINISH, 2, 1),
 )
 
 
@@ -190,7 +193,7 @@
     pltpu.make_async_copy(rest, rest, x_r.at[1 - core]).wait()
     for g in range(GROUPS):
         for h in range(2):
-            xg[g, y, h] = (
+            xg[0, g, y, h] = (
                 x_dst[h, g * 8 : (g + 1) * 8].astype(F32).reshape(TILE, CH).astype(BF16)
             )
 
@@ -200,9 +203,9 @@
         (y, 1, to_left), (y, 0, to_left), (right, 1, to_left),
     )
 
-    def ag(g, k):
+    def ag(l, g, k):
         owner, half, target = gather[k]
-        ref = xg.at[g, owner, half]
+        ref = xg.at[l, g, owner, half]
         return remote(ref, ref, ag_s.at[g, k], ag_r.at[g, k], {"tp": target})
 
     sides = (opp, right, left, y)
@@ -217,33 +220,30 @@
             ssum.at[g, side, half], rs_y.at[g, k], y_s.at[g, k], y_r.at[g, k], {"tp": target}
         )
 
-    def halo(par, g, k):
+    def halo(l, g, k):
         slot = 2 * core if k else 2 * (1 - core)
         target = {"tp": partner}
         if k == 0:
             target["sp"] = (sp + 2 * core - 1 + n_sp) % n_sp
-        return remote(kv.at[par, 1, g], kv.at[par, slot, g], h_s.at[par, g, k], h_r.at[par, g, k], target)
+        return remote(kv.at[l, 1, g], kv.at[l, slot, g], h_s.at[l, g, k], h_r.at[l, g, k], target)
 
     lane_head = lax.broadcasted_iota(jnp.int32, (TILE, CH), 1) // HEAD_DIM
     head_mask = [(lane_head == h).astype(F32).astype(BF16) for h in range(4)]
 
-    def start_own(g):
+    def step_own(l, g):
         for k in (0, 3, 1, 4):
-            ag(g, k).start()
-
-    def step_own(l, g):
-        start_own(g)
+            ag(l, g, k).start()
 
     def step_relay(l, g):
         for k, onward in ((0, 2), (3, 5)):
-            ag(g, k).wait_recv()
-            ag(g, onward).start()
+            ag(l, g, k).wait_recv()
+            ag(l, g, onward).start()
 
     def accumulate(l, g, blocks, fresh):
         total = None
         squares = None
         for chip, half in blocks:
-            wide = xg[g, chip, half].astype(F32)
+            wide = xg[l, g, chip, half].astype(F32)
             sq_b = wide * wide
             sq_b = sq_b[:, :128] + sq_b[:, 128:]
             squares = sq_b if squares is None else squares + sq_b
@@ -272,57 +272,62 @@
         accumulate(l, g, ((y, 0), (y, 1)), True)
 
     def step_sides(l, g):
-        ag(g, 1).wait_recv()
-        ag(g, 4).wait_recv()
+        ag(l, g, 1).wait_recv()
+        ag(l, g, 4).wait_recv()
         accumulate(l, g, ((left, 0), (right, 1), (left, 1), (right, 0)), False)
 
     def step_far(l, g):
-        par = l % 2
-        ag(g, 2).wait_recv()
-        ag(g, 5).wait_recv()
-        accumulate(l, g, ((opp, 0), (opp, 1)), False)
-        inverse = lax.rsqrt(jnp.sum(sq[g], axis=1, keepdims=True) / D + EPS)
-        if l >= 2:
-            for k in range(2):
-                halo(par, g, k).wait_send()
-        kv[par, 1, g] = (acc[g, :, PAIR:] * inverse).astype(BF16)
+        ag(l, g, 2).wait_recv()
+        ag(l, g, 5).wait_recv()
+        squares = sq[g]
+        scaled = []
+        for half in range(2):
+            wide = xg[l, g, opp, half].astype(F32)
+            scaled.append((wide * gains[l, opp * 2 + half]).astype(BF16))
+            wide = wide * wide
+            squares = squares + wide[:, :128] + wide[:, 128:]
+        inverse = lax.rsqrt(jnp.sum(squares, axis=1, keepdims=True) / D + EPS)
+
+        def total(lo, hi):
+            return acc[g, :, lo:hi] + (
+                dot(scaled[0], wqkv[l, opp * 2, :, lo:hi])
+                + dot(scaled[1], wqkv[l, opp * 2 + 1, :, lo:hi])
+            )
+
+        kv[l, 1, g] = (total(PAIR, 3 * PAIR) * inverse).astype(BF16)
         for k in range(2):
-            halo(par, g, k).start()
-        qs[g] = (acc[g, :, :PAIR] * (inverse * HEAD_DIM**-0.5)).astype(BF16)
+            halo(l, g, k).start()
+        qs[g] = (total(0, PAIR) * (inverse * HEAD_DIM**-0.5)).astype(BF16)
         for k in range(6):
-            ag(g, k).wait_send()
-
-    def window(par, slot, g, lo):
-        up, down = (g + 3) % 4, (g + 1) % 4
+            ag(l, g, k).wait_send()
+
+    def window(l, slot, g, lo):
         return jnp.concatenate(
-            [
-                kv[par, slot, up, TILE // 2 :, lo : lo + CH],
-                kv[par, slot, g, :, lo : lo + CH],
-                kv[par, slot, down, : TILE // 2, lo : lo + CH],
-            ],
-            axis=0,
+            [kv[l, slot, g, :, lo : lo + CH], kv[l, slot, (g + 1) % 4, :, lo : lo + CH]], axis=0
         )
 
     def step_attend(l, g):
-        par = l % 2
-        for near in ((g + 3) % 4, g, (g + 1) % 4):
+        after = (g + 1) % 4
+        for near in (g, after):
             if (l, near, "halo") not in ready:
                 ready.add((l, near, "halo"))
                 for k in range(2):
-                    halo(par, near, k).wait_recv()
+                    halo(l, near, k).wait_recv()
         for c in range(2):
             lo = c * CH
-            q = qs[g, :, lo : lo + CH]
+            q = jnp.concatenate(
+                [qs[g, TILE // 2 :, lo : lo + CH], qs[after, : TILE // 2, lo : lo + CH]], axis=0
+            )
             q_all = jnp.concatenate([q * m for m in head_mask], axis=0)
             table = bias[l, 4 * c : 4 * c + 4].reshape(4 * TILE, 3 * 128)
             scores = jnp.concatenate(
-                [dot_nt(q_all, window(par, j, g, lo)) for j in range(3)], axis=1
+                [dot_nt(q_all, window(l, j, g, lo)) for j in range(3)], axis=1
             ) + table
             highest = jnp.max(scores, axis=1, keepdims=True)
             weights = jnp.exp(scores - highest)
             total = jnp.sum(weights, axis=1, keepdims=True)
             weights = weights.astype(BF16)
-            values = jnp.concatenate([window(par, j, g, PAIR + lo) for j in range(3)], axis=0)
+            values = jnp.concatenate([window(l, j, g, PAIR + lo) for j in range(3)], axis=0)
             o = dot(weights, values) / total
             out = o[:TILE]
             for h in range(1, 4):
@@ -333,18 +338,29 @@
             for i in range(parts):
                 weights_across(l + 1, i).start()
 
-    def step_project(l, g):
+    def chunk(l, g, k):
+        piece = dot(mixed[g], wout[l, sides[k]])
+        return piece[:, :CH], piece[:, CH:]
+
+    def step_first(l, g):
         weights_in(l, 1, range(3, parts))
-        m = mixed[g]
-        for k in range(3):
-            piece = dot(m, wout[l, sides[k]]).astype(BF16)
-            for half in range(2):
-                ssum[g, k, half] = piece[:, half * CH : (half + 1) * CH]
-        for k in range(4):
-            ring(g, k).start()
-        piece = dot(m, wout[l, y])
-        for half in range(2):
-            own[g, half] = piece[:, half * CH : (half + 1) * CH] + xg[g, y, half].astype(F32)
+        for half, piece in enumerate(chunk(l, g, 0)):
+            ssum[g, 0, half] = piece.astype(BF16)
+        ring(g, 0).start()
+        ring(g, 1).start()
+
+    def step_rest(l, g):
+        for k in (1, 2):
+            for half, piece in enumerate(chunk(l, g, k)):
+                ssum[g, k, half] = piece.astype(BF16)
+        ring(g, 2).start()
+        ring(g, 3).start()
+        after = (g + 1) % 4
+        for half, piece in enumerate(chunk(l, g, 3)):
+            before = jnp.concatenate(
+                [xg[l, g, y, half, TILE // 2 :], xg[l, after, y, half, : TILE // 2]], axis=0
+            )
+            own[g, half] = piece + before.astype(F32)
 
     def step_add(l, g):
         for k in range(2):
@@ -362,29 +378,30 @@
         )
         if l < LAYERS - 1:
             for half in range(2):
-                xg[g, y, half] = new[half].astype(BF16)
-            start_own(g)
+                xg[l + 1, g, y, half] = new[half].astype(BF16)
+            step_own(l + 1, g)
         else:
             for half in range(2):
                 o_src[half, 8 * g : 8 * g + 8] = new[half].reshape(8, STRIP_C, CH).astype(BF16)
 
             def send(r, carry):
-                row = 8 * g + r
+                slot = 8 * g + r
+                row = (slot + LAYERS * WIN_R // 2) % ROWS
                 there, spot = row // rows, row % rows
 
                 @pl.when(there != sp)
                 def _():
                     remote(
-                        o_src.at[core, row], o_dst.at[core, sp, spot], o_s.at[0], o_r.at[core],
+                        o_src.at[core, slot], o_dst.at[core, sp, spot], o_s.at[0], o_r.at[core],
                         {"sp": there},
                     ).start()
 
                 @pl.when(there == sp)
                 def _():
-                    o_dst[core, sp, spot] = o_src[core, row]
+                    o_dst[core, sp, spot] = o_src[core, slot]
 
                 remote(
-                    o_src.at[1 - core, row], o_dst.at[core, sp, spot], o_s.at[1], o_r.at[core],
+                    o_src.at[1 - core, slot], o_dst.at[core, sp, spot], o_s.at[1], o_r.at[core],
                     {"sp": there, "tp": partner},
                 ).start()
                 return carry
@@ -395,7 +412,7 @@
 
     steps = (
         step_own, step_relay, step_mine, step_sides, step_far,
-        step_attend, step_project, step_add, step_finish,
+        step_attend, step_first, step_rest, step_add, step_finish,
     )
     for step, l, g in ORDER:
         steps[step](l, g)
@@ -403,10 +420,10 @@
     for l in range(LAYERS):
         for i in range(parts):
             weights_across(l, i).wait_send()
-    for l in range(1, LAYERS):
+    for l in range(LAYERS):
         for g in range(GROUPS):
             for k in range(2):
-                halo(l % 2, g, k).wait_send()
+                halo(l, g, k).wait_send()
     gone = x_src.at[pl.ds(0, n_sp - 1), core]
     pltpu.make_async_copy(gone, gone, x_s.at[0]).wait()
     gone = x_src.at[:, core]
@@ -448,11 +465,11 @@
             pltpu.VMEM((2, LAYERS, 4, WIN_R, WIN_C), F32),
             pltpu.VMEM((LAYERS, HEADS, WIN_R, 128), F32),
             pltpu.VMEM((LAYERS, HEADS, TILE, 3 * 128), F32),
-            pltpu.VMEM((GROUPS, CHIPS, 2, TILE, CH), BF16),
+            pltpu.VMEM((LAYERS, GROUPS, CHIPS, 2, TILE, CH), BF16),
             pltpu.VMEM((GROUPS, TILE, 3 * PAIR), F32),
             pltpu.VMEM((GROUPS, TILE, 128), F32),
             pltpu.VMEM((GROUPS, TILE, PAIR), BF16),
-            pltpu.VMEM((2, 3, GROUPS, TILE, 2 * PAIR), BF16),
+            pltpu.VMEM((LAYERS, 3, GROUPS, TILE, 2 * PAIR), BF16),
             pltpu.VMEM((GROUPS, TILE, PAIR), BF16),
             pltpu.VMEM((GROUPS, 3, 2, TILE, CH), BF16),
             pltpu.VMEM((GROUPS, 2, TILE, CH), F32),
@@ -460,7 +477,7 @@
             dma((LAYERS, parts)), dma((LAYERS, parts)), dma((LAYERS, parts)),
             dma((1,)), dma((1,)), dma((2,)), dma((2,)), dma((2,)), dma((2,)),
             dma((GROUPS, 6)), dma((GROUPS, 6)), dma((GROUPS, 6)), dma((GROUPS, 6)),
-            dma((2, GROUPS, 2)), dma((2, GROUPS, 2)),
+            dma((LAYERS, GROUPS, 2)), dma((LAYERS, GROUPS, 2)),
         ],
         compiler_params=pltpu.CompilerParams(
             collective_id=0, has_side_effects=True, vmem_limit_bytes=60 * 1024 * 1024

time: 113 us -> 108 us (0.956)
  Pallas kernels: 111 us -> 106 us
    pallas_call x1, Pallas kernels: 111 us -> 106 us  [body(): pl.pallas_call(functools.partial(kernel, n_sp, rows), out_shape=jax.Shape...]
where the time goes in v4:
time: 108 us
  Pallas kernels  106 us (98%)
  local copies, waits for them, and re-layouts  1.67 us (2%)
    pallas_call x1, Pallas kernels, body(): pl.pallas_call(functools.partial(kernel, n_sp, rows), out_shape=jax.Shape...  106 us

profile of v4, /device:TPU:1, one launch (start us, length us, event | category | flops | bytes accessed | tf_op | source)
XLA Modules:
  0.0 107.8 jit_solution(14271002370890045652)
XLA Ops:
  0.0 106.1 %shard_map.73 = bf16[1,256,512]{2,1,0:T(8,128)(2,1)} custom-call(bf16[1,256,512]{2,1,0:T(8,128)(2,1)} %x_ref.1, bf16[3,2048]{1,0:T(4,128)(2,1)} %gain_ref.1, f32[3,4,8,16]{3,2,1,0:T(8,128)} %bias_ref.1, bf16[3,8,256,256]{3,2,1,0:T(8,128)(2,1)} %bitcast.3, bf16[3,8,256,256]{3,2,1,0:T(8,128)(2,1)} %bitcast.4, bf16[3,8,256,256]{3,2,1,0:T(8,128)(2,1)} %bitcast.5, ...), custom_call_target="tpu_custom_call" | custom-call | tf_op jit(solution)/shard_map/pallas_call | solution.py:452
  106.1 1.7 %copy.9 = bf16[1,256,512]{2,1,0:T(8,128)(2,1)} copy(bf16[1,256,512]{2,1,0:T(8,128)(2,1)} %shard_map.73) | data formatting | bytes 524288

commit v5 on v4

--- a/solution.py
+++ b/solution.py
@@ -228,6 +228,7 @@
         return remote(kv.at[l, 1, g], kv.at[l, slot, g], h_s.at[l, g, k], h_r.at[l, g, k], target)
 
     lane_head = lax.broadcasted_iota(jnp.int32, (TILE, CH), 1) // HEAD_DIM
+    ones = jnp.ones((3 * 128, 128), BF16)
     head_mask = [(lane_head == h).astype(F32).astype(BF16) for h in range(4)]
 
     def step_own(l, g):
@@ -313,6 +314,7 @@
                 ready.add((l, near, "halo"))
                 for k in range(2):
                     halo(l, near, k).wait_recv()
+        scores, values = [], []
         for c in range(2):
             lo = c * CH
             q = jnp.concatenate(
@@ -320,19 +322,23 @@
             )
             q_all = jnp.concatenate([q * m for m in head_mask], axis=0)
             table = bias[l, 4 * c : 4 * c + 4].reshape(4 * TILE, 3 * 128)
-            scores = jnp.concatenate(
-                [dot_nt(q_all, window(l, j, g, lo)) for j in range(3)], axis=1
-            ) + table
-            highest = jnp.max(scores, axis=1, keepdims=True)
-            weights = jnp.exp(scores - highest)
-            total = jnp.sum(weights, axis=1, keepdims=True)
-            weights = weights.astype(BF16)
-            values = jnp.concatenate([window(l, j, g, PAIR + lo) for j in range(3)], axis=0)
-            o = dot(weights, values) / total
+            scores.append(
+                [dot_nt(q_all, window(l, j, g, lo)) + table[:, j * 128 : (j + 1) * 128] for j in range(3)]
+            )
+            values.append([window(l, j, g, PAIR + lo) for j in range(3)])
+        highest = [
+            jnp.max(jnp.maximum(jnp.maximum(s[0], s[1]), s[2]), axis=1, keepdims=True) for s in scores
+        ]
+        weights = [[jnp.exp(s - top).astype(BF16) for s in ss] for ss, top in zip(scores, highest)]
+        for c in range(2):
+            wide = jnp.concatenate(weights[c], axis=1)
+            total = dot(wide, ones)
+            o = dot(wide, jnp.concatenate(values[c], axis=0))
+            o = o * (1.0 / jnp.concatenate([total, total], axis=1))
             out = o[:TILE]
             for h in range(1, 4):
                 out = jnp.where(lane_head == h, o[h * TILE : (h + 1) * TILE], out)
-            mixed[g, :, lo : lo + CH] = out.astype(BF16)
+            mixed[g, :, c * CH : (c + 1) * CH] = out.astype(BF16)
         if l < LAYERS - 1 and (l, "across") not in ready:
             ready.add((l, "across"))
             for i in range(parts):
@@ -446,7 +452,7 @@
     rows = token_grid.shape[0]
     wq, wk, wv = (w.reshape(LAYERS, N_TP, CH, CH) for w in (w_query, w_key, w_value))
     vmem = pl.BlockSpec(memory_space=pltpu.VMEM)
-    hbm = pl.BlockSpec(memory_space=pl.ANY)
+    hbm = pl.BlockSpec(memory_space=pltpu.HBM)
     dma = pltpu.SemaphoreType.DMA
     parts = 3 + CHIPS
     return pl.pallas_call(
@@ -480,7 +486,7 @@
             dma((LAYERS, GROUPS, 2)), dma((LAYERS, GROUPS, 2)),
         ],
         compiler_params=pltpu.CompilerParams(
-            collective_id=0, has_side_effects=True, vmem_limit_bytes=60 * 1024 * 1024
+            collective_id=0, has_side_effects=True, vmem_limit_bytes=52 * 1024 * 1024
         ),
     )(token_grid, norm_gain, rel_bias, wq, wk, wv, w_out)
 

time: 108 us -> 107 us (level)
  Pallas kernels: 106 us -> 103 us
  local copies, waits for them, and re-layouts: 1.67 us -> 3.17 us
    pallas_call x1, Pallas kernels: 106 us -> 103 us  [body(): pl.pallas_call(functools.partial(kernel, n_sp, rows), out_shape=jax.Shape...]
    unnamed x1 -> x7, local copies, waits for them, and re-layouts: 1.67 us -> 3.17 us
where the time goes in v5:
time: 107 us
  Pallas kernels  103 us (96%)
  local copies, waits for them, and re-layouts  3.17 us (3%)
    pallas_call x1, Pallas kernels, body(): pl.pallas_call(functools.partial(kernel, n_sp, rows), out_shape=jax.Shape...  103 us
    unnamed x7, local copies, waits for them, and re-layouts  3.17 us

profile of v5, /device:TPU:1, one launch (start us, length us, event | category | flops | bytes accessed | tf_op | source)
XLA Modules:
  0.0 106.6 jit_solution(2808535754685456920)
XLA Ops:
  0.0 0.0 copy-start
  0.0 0.9 copy-done
  1.0 0.0 copy-start.1
  1.0 0.8 copy-done.1
  1.8 0.0 copy-start.2
  1.8 0.7 copy-done.2
  2.5 103.4 %shard_map.73 = bf16[1,256,512]{2,1,0:T(8,128)(2,1)S(1)} custom-call(bf16[1,256,512]{2,1,0:T(8,128)(2,1)S(1)} %copy-done, bf16[3,2048]{1,0:T(4,128)(2,1)S(1)} %copy-done.2, f32[3,4,8,16]{3,2,1,0:T(8,128)S(1)} %copy-done.1, bf16[3,8,256,256]{3,2,1,0:T(8,128)(2,1)} %bitcast.3, bf16[3,8,256,256]{3,2,1,0:T(8,128)(2,1)} %bitcast.4, ...), custom_call_target="tpu_custom_call" | custom-call | tf_op jit(solution)/shard_map/pallas_call | solution.py:458
  105.8 0.7 copy.9
Async XLA Ops:
  0.0 0.9 copy-start
  1.0 0.8 copy-start.1
  1.8 0.7 copy-start.2

commit v6 on v5

--- a/solution.py
+++ b/solution.py
@@ -29,26 +29,26 @@
 
 OWN, RELAY, MINE, SIDES, FAR, ATTEND, FIRST, REST, ADD, FINISH = range(10)
 ORDER = (
-    (OWN, 0, 2), (OWN, 0, 3), (OWN, 0, 0), (OWN, 0, 1), (MINE, 0, 2),
-    (MINE, 0, 3), (MINE, 0, 0), (RELAY, 0, 2), (SIDES, 0, 2), (RELAY, 0, 3),
-    (SIDES, 0, 3), (RELAY, 0, 0), (SIDES, 0, 0), (RELAY, 0, 1), (MINE, 0, 1),
-    (SIDES, 0, 1), (FAR, 0, 2), (FAR, 0, 3), (FAR, 0, 0), (FAR, 0, 1),
-    (ATTEND, 0, 2), (FIRST, 0, 2), (REST, 0, 2), (ATTEND, 0, 3), (FIRST, 0, 3),
-    (REST, 0, 3), (ATTEND, 0, 0), (FIRST, 0, 0), (ADD, 0, 2), (REST, 0, 0),
-    (ATTEND, 0, 1), (FIRST, 0, 1), (ADD, 0, 3), (REST, 0, 1), (ADD, 0, 0),
-    (FINISH, 0, 2), (MINE, 1, 2), (ADD, 0, 1), (FINISH, 0, 3), (MINE, 1, 3),
-    (RELAY, 1, 2), (FINISH, 0, 0), (MINE, 1, 0), (SIDES, 1, 2), (RELAY, 1, 3),
-    (FINISH, 0, 1), (SIDES, 1, 3), (FAR, 1, 2), (RELAY, 1, 0), (SIDES, 1, 0),
-    (FAR, 1, 3), (RELAY, 1, 1), (FAR, 1, 0), (MINE, 1, 1), (SIDES, 1, 1),
-    (FAR, 1, 1), (ATTEND, 1, 2), (FIRST, 1, 2), (REST, 1, 2), (ATTEND, 1, 3),
-    (FIRST, 1, 3), (REST, 1, 3), (ADD, 1, 2), (ATTEND, 1, 0), (FIRST, 1, 0),
-    (REST, 1, 0), (ADD, 1, 3), (ATTEND, 1, 1), (FIRST, 1, 1), (FINISH, 1, 2),
-    (MINE, 2, 2), (ADD, 1, 0), (REST, 1, 1), (FINISH, 1, 3), (ADD, 1, 1),
-    (MINE, 2, 3), (RELAY, 2, 2), (FINISH, 1, 0), (MINE, 2, 0), (SIDES, 2, 2),
-    (RELAY, 2, 3), (FINISH, 1, 1), (MINE, 2, 1), (FAR, 2, 2), (RELAY, 2, 0),
-    (SIDES, 2, 3), (SIDES, 2, 0), (RELAY, 2, 1), (FAR, 2, 3), (SIDES, 2, 1),
-    (FAR, 2, 0), (FAR, 2, 1), (ATTEND, 2, 2), (FIRST, 2, 2), (REST, 2, 2),
-    (ATTEND, 2, 3), (FIRST, 2, 3), (REST, 2, 3), (ATTEND, 2, 0), (FIRST, 2, 0),
+    (OWN, 0, 0), (OWN, 0, 3), (MINE, 0, 0), (MINE, 0, 3), (OWN, 0, 1),
+    (OWN, 0, 2), (MINE, 0, 1), (MINE, 0, 2), (RELAY, 0, 0), (SIDES, 0, 0),
+    (RELAY, 0, 3), (SIDES, 0, 3), (RELAY, 0, 1), (SIDES, 0, 1), (RELAY, 0, 2),
+    (SIDES, 0, 2), (FAR, 0, 0), (FAR, 0, 3), (FAR, 0, 1), (FAR, 0, 2),
+    (ATTEND, 0, 3), (FIRST, 0, 3), (REST, 0, 3), (ATTEND, 0, 0), (FIRST, 0, 0),
+    (REST, 0, 0), (ATTEND, 0, 1), (FIRST, 0, 1), (REST, 0, 1), (ADD, 0, 3),
+    (ATTEND, 0, 2), (FIRST, 0, 2), (ADD, 0, 0), (REST, 0, 2), (ADD, 0, 1),
+    (FINISH, 0, 3), (MINE, 1, 3), (ADD, 0, 2), (FINISH, 0, 0), (MINE, 1, 0),
+    (FINISH, 0, 1), (MINE, 1, 1), (RELAY, 1, 3), (SIDES, 1, 3), (FINISH, 0, 2),
+    (MINE, 1, 2), (RELAY, 1, 0), (SIDES, 1, 0), (RELAY, 1, 1), (SIDES, 1, 1),
+    (FAR, 1, 3), (RELAY, 1, 2), (SIDES, 1, 2), (FAR, 1, 0), (FAR, 1, 1),
+    (FAR, 1, 2), (ATTEND, 1, 3), (FIRST, 1, 3), (REST, 1, 3), (ATTEND, 1, 0),
+    (FIRST, 1, 0), (REST, 1, 0), (ATTEND, 1, 2), (FIRST, 1, 2), (REST, 1, 2),
+    (ADD, 1, 3), (ATTEND, 1, 1), (FIRST, 1, 1), (ADD, 1, 0), (REST, 1, 1),
+    (ADD, 1, 2), (FINISH, 1, 3), (MINE, 2, 3), (ADD, 1, 1), (FINISH, 1, 0),
+    (MINE, 2, 0), (FINISH, 1, 2), (MINE, 2, 2), (RELAY, 2, 3), (SIDES, 2, 3),
+    (FINISH, 1, 1), (MINE, 2, 1), (RELAY, 2, 0), (SIDES, 2, 0), (RELAY, 2, 2),
+    (SIDES, 2, 2), (FAR, 2, 3), (RELAY, 2, 1), (SIDES, 2, 1), (FAR, 2, 0),
+    (FAR, 2, 2), (FAR, 2, 1), (ATTEND, 2, 3), (FIRST, 2, 3), (REST, 2, 3),
+    (ATTEND, 2, 2), (FIRST, 2, 2), (REST, 2, 2), (ATTEND, 2, 0), (FIRST, 2, 0),
     (REST, 2, 0), (ATTEND, 2, 1), (FIRST, 2, 1), (REST, 2, 1), (ADD, 2, 2),
     (ADD, 2, 3), (ADD, 2, 0), (ADD, 2, 1), (FINISH, 2, 2), (FINISH, 2, 3),
     (FINISH, 2, 0), (FINISH, 2, 1),

time: 107 us -> 106 us (level)
  no operation moved by 1% of the time
where the time goes in v6:
time: 106 us
  Pallas kernels  102 us (96%)
  local copies, waits for them, and re-layouts  3.17 us (3%)
    pallas_call x1, Pallas kernels, body(): pl.pallas_call(functools.partial(kernel, n_sp, rows), out_shape=jax.Shape...  102 us
    unnamed x7, local copies, waits for them, and re-layouts  3.17 us

profile of v6, /device:TPU:1, one launch (start us, length us, event | category | flops | bytes accessed | tf_op | source)
XLA Modules:
  0.0 105.7 jit_solution(2849140834098326011)
XLA Ops:
  0.0 0.0 copy-start
  0.0 0.9 copy-done
  1.0 0.0 copy-start.1
  1.0 0.8 copy-done.1
  1.8 0.0 copy-start.2
  1.8 0.7 copy-done.2
  2.5 102.5 %shard_map.73 = bf16[1,256,512]{2,1,0:T(8,128)(2,1)S(1)} custom-call(bf16[1,256,512]{2,1,0:T(8,128)(2,1)S(1)} %copy-done, bf16[3,2048]{1,0:T(4,128)(2,1)S(1)} %copy-done.2, f32[3,4,8,16]{3,2,1,0:T(8,128)S(1)} %copy-done.1, bf16[3,8,256,256]{3,2,1,0:T(8,128)(2,1)} %bitcast.3, bf16[3,8,256,256]{3,2,1,0:T(8,128)(2,1)} %bitcast.4, ...), custom_call_target="tpu_custom_call" | custom-call | tf_op jit(solution)/shard_map/pallas_call | solution.py:458
  105.0 0.7 copy.9
Async XLA Ops:
  0.0 0.9 copy-start
  1.0 0.8 copy-start.1
  1.8 0.7 copy-start.2
